TPU v7x, 256 devices: a whole 4x4x8 slice. The times are simulated.
256 devices in a mesh: ep: 64 (over z, y, core), tp: 4 (over x).
Axes of the slice: x: 4, y: 4, z: 8, core: 2. Of those that a mesh axis runs over, the one named last changes fastest.
Arguments:
- queries: bfloat16 [12288, 8, 128], P('ep', 'tp'), may hold values from -140 to 140
- keys: bfloat16 [12288, 4, 128], P('ep', 'tp'), may hold values from -6 to 6
- values: bfloat16 [12288, 4, 128], P('ep', 'tp'), may hold values from -6 to 6
- mix_scale: float32 [8], P('tp'), may hold values from 0.3 to 0.8
- head_gain: float32 [128], replicated, may hold values from 0.1 to 1.9
- out_weight: bfloat16 [8, 128, 2048], P('tp'), may hold values from -0.1875 to 0.1875
- moe_input: bfloat16 [24576, 2048], P(('ep', 'tp')), may hold values from -6 to 6
- norm_gain: float32 [2048], replicated, may hold values from 0.1 to 1.9
- routes: int32 [24576, 2], P(('ep', 'tp')), may hold values from 0 to 63, all different within a row; in each aligned block of 96 rows (0 to 95, 96 to 191, ...) at most 4 rows name the same one
- route_weights: float32 [24576, 2], P(('ep', 'tp')), may hold values from 0.2 to 1
- gate_weight: bfloat16 [64, 2048, 3584], P('ep', None, 'tp'), may hold values from -0.125 to 0.125
- up_weight: bfloat16 [64, 2048, 3584], P('ep', None, 'tp'), may hold values from -0.125 to 0.125
- down_weight: bfloat16 [64, 3584, 2048], P('ep', 'tp'), may hold values from -0.09375 to 0.09375
Outputs:
- attn_out: bfloat16 [12288, 2048], P(('ep', 'tp'))
- moe_out: bfloat16 [24576, 2048], P(('ep', 'tp'))
Inputs may be any that keep to these rules, and one draw needn't show every extreme that they name: `routes`: the 2 experts of a row differ. In each aligned block of 96 rows (the rows of one device) no expert is named by more than 4 rows, and in some blocks an expert is named by exactly 4 rows.
All inputs are finite; a program needn't handle non-finite values.
Results may differ from a plain program's by a relative error of at most 0.014.
Values may be sent and summed in bfloat16 or wider, within the bound.
A program may use at most 128 MiB of HBM per device.

v0:
```python
import math

import jax
import jax.numpy as jnp
from jax import lax
from jax.sharding import Mesh
from jax.sharding import PartitionSpec as P

EP = ("ep_0", "ep_1", "ep_2")
EP_TP = ("ep_0", "ep_1", "ep_2", "tp")


NEG_LARGE = -1e30


def joined_along(tiles, dim):
    tiles = jnp.moveaxis(tiles, 0, dim)
    lengths = tiles.shape
    return tiles.reshape(*lengths[:dim], lengths[dim] * lengths[dim + 1], *lengths[dim + 2 :])


def gather_in_order(value, axes, order):
    tiles = value[None]
    for k in order:
        tiles = lax.all_gather(tiles, axes[k], axis=0, tiled=True)
    current = [lax.axis_size(axes[k]) for k in reversed(order)]
    tiles = tiles.reshape(*current, *value.shape)
    turned = sorted(range(len(order)), key=lambda place: order[len(order) - 1 - place])
    return tiles.transpose(*turned, *range(len(order), tiles.ndim)).reshape(-1, *value.shape)


def gathered_by_axis(value, axes, order, dim):
    return joined_along(gather_in_order(value, axes, order), dim)


def split_up(value, dim, peers):
    before, after = (value.shape[:dim], value.shape[dim + 1 :])
    return jnp.moveaxis(value.reshape(*before, peers, -1, *after), dim, 0)


def summed_on_arrival(value, axis, dim):
    peers = lax.axis_size(axis)
    tiles = lax.all_to_all(split_up(value, dim, peers), axis, 0, 0, tiled=True)
    return jnp.sum(tiles.astype(jnp.float32), axis=0)


def attend_update(running, query_set, positions, key_block, value_block, key_anchor, scaling):
    row_peak, totals, numerator = running
    span = key_block.shape[0]
    scores = (
        jnp.einsum("tkgmd,skmd->kgmts", query_set, key_block, preferred_element_type=jnp.float32)
        * scaling
    )
    visible = (key_anchor + jnp.arange(span, dtype=jnp.int32))[None, :] <= positions[:, None]
    scores = jnp.where(visible, scores, NEG_LARGE)
    new_peak = jnp.maximum(row_peak, jnp.max(scores, axis=-1))
    weights = jnp.where(visible, jnp.exp(scores - new_peak[..., None]), 0.0)
    factor = jnp.exp(row_peak - new_peak)
    totals = totals * factor + jnp.sum(weights, axis=-1)
    numerator = numerator * factor[..., None] + jnp.einsum(
        "rnouf,frj->rnouj",
        weights.astype(jnp.bfloat16),
        value_block,
        preferred_element_type=jnp.float32,
    )
    return (new_peak, totals, numerator)


def body(
    queries,
    keys,
    values,
    mix_scale,
    head_gain,
    out_weight,
    moe_input,
    norm_gain,
    routes,
    route_weights,
    gate_weight,
    up_weight,
    down_weight,
):
    rows_here = queries.shape[0]
    key_heads = keys.shape[1]
    head_count = queries.shape[1]
    group_size = head_count // key_heads
    head_dim = queries.shape[2] // 2
    value_dim = values.shape[2]
    ep_size = lax.axis_size(EP)
    own_start = lax.axis_index(EP) * rows_here
    grouped = queries.reshape(rows_here, key_heads, group_size, 2, head_dim)
    own_positions = own_start + jnp.arange(rows_here, dtype=jnp.int32)
    query_sets = ((grouped, own_positions),)
    scaling = 1.0 / math.sqrt(head_dim)

    def empty_state(row_total):
        return (
            jnp.full((key_heads, group_size, 2, row_total), NEG_LARGE, jnp.float32),
            jnp.zeros((key_heads, group_size, 2, row_total), jnp.float32),
            jnp.zeros((key_heads, group_size, 2, row_total, value_dim), jnp.float32),
        )

    initial = tuple((empty_state(entry[0].shape[0]) for entry in query_sets))
    key_rows = gathered_by_axis(keys, EP, (1, 0, 2), 0)
    value_rows = gathered_by_axis(values, EP, (1, 0, 2), 0)
    length = key_rows.shape[0]
    span = length
    while span > 1024 and span % 2 == 0:
        span = span // 2
    key_rows = key_rows.reshape(length, key_heads, 2, head_dim)

    def sweep(step_id, states):
        anchor = step_id * span
        key_block = lax.dynamic_slice_in_dim(key_rows, step_id * span, span, 0)
        value_block = lax.dynamic_slice_in_dim(value_rows, step_id * span, span, 0)
        updated = []
        for (query_set, positions), status in zip(query_sets, states):

            def advance(current):
                return attend_update(
                    current, query_set, positions, key_block, value_block, anchor, scaling
                )

            def unchanged(current):
                return current

            updated.append(lax.cond(anchor <= positions[-1], advance, unchanged, status))
        return tuple(updated)

    folded = lax.fori_loop(0, length // span, sweep, initial)
    mixing = mix_scale.reshape(key_heads, group_size, 1, 1)
    outputs = []
    for status in folded:
        row_peak, totals, numerator = status
        blended = numerator[:, :, 0] / totals[:, :, 0, :, None] - mixing * (
            numerator[:, :, 1] / totals[:, :, 1, :, None]
        )
        normed = (
            blended
            * lax.rsqrt(jnp.mean(blended * blended, axis=-1, keepdims=True) + 1e-05)
            * head_gain
        )
        outputs.append(
            jnp.transpose(normed.astype(jnp.bfloat16), (2, 0, 1, 3)).reshape(
                -1, head_count * value_dim
            )
        )
    head_flat = outputs[0]
    weight_flat = out_weight.reshape(head_count * value_dim, -1)
    widened = moe_input.astype(jnp.float32)
    normed_in = (
        widened * lax.rsqrt(jnp.mean(widened * widened, axis=-1, keepdims=True) + 1e-06) * norm_gain
    ).astype(jnp.bfloat16)
    tok_count = moe_input.shape[0]
    top_count = routes.shape[1]
    experts = ep_size * gate_weight.shape[0]
    capacity = max(2, 3 * top_count * tok_count // (2 * experts))
    flattened = routes.reshape(-1)
    one_hot = (flattened[:, None] == jnp.arange(experts, dtype=jnp.int32)[None, :]).astype(
        jnp.int32
    )
    before = jnp.cumsum(one_hot, axis=0) - one_hot
    ranking = jnp.sum(before * one_hot, axis=1)
    slot_ids = (flattened * capacity + ranking).reshape(tok_count, top_count)
    slot_total = experts * capacity
    dispatch = jnp.any(
        jnp.arange(slot_total, dtype=jnp.int32)[:, None, None] == slot_ids[None], axis=2
    ).astype(jnp.bfloat16)
    outbound = jnp.dot(dispatch, normed_in, preferred_element_type=jnp.float32).astype(jnp.bfloat16)
    received = lax.all_to_all(outbound, EP, split_axis=0, concat_axis=0, tiled=True)
    inputs = lax.all_gather(received, "tp", axis=0, tiled=True)
    gate_proj = jnp.dot(inputs, gate_weight[0], preferred_element_type=jnp.float32)
    up_proj = jnp.dot(inputs, up_weight[0], preferred_element_type=jnp.float32)
    hidden_all = (jax.nn.silu(gate_proj) * up_proj).astype(jnp.bfloat16)
    attn_out = summed_on_arrival(
        jnp.dot(head_flat, weight_flat, preferred_element_type=jnp.float32).astype(jnp.bfloat16),
        "tp",
        0,
    ).astype(jnp.bfloat16)
    expert_out = summed_on_arrival(
        jnp.dot(hidden_all, down_weight[0], preferred_element_type=jnp.float32).astype(
            jnp.bfloat16
        ),
        "tp",
        0,
    ).astype(jnp.bfloat16)
    returned_rows = lax.all_to_all(expert_out, EP, split_axis=0, concat_axis=0, tiled=True)
    picked = jnp.take(returned_rows, slot_ids, axis=0)
    moe_out = jnp.sum(route_weights[:, :, None] * picked.astype(jnp.float32), axis=1).astype(
        jnp.bfloat16
    )
    return (attn_out, moe_out)


def solution(mesh):
    split = Mesh(mesh.devices.reshape(8, 4, 2, mesh.shape["tp"]), ("ep_0", "ep_1", "ep_2", "tp"))
    placed = (
        P(EP, "tp", None),
        P(EP, "tp", None),
        P(EP, "tp", None),
        P("tp"),
        P(),
        P("tp", None, None),
        P(EP_TP, None),
        P(),
        P(EP_TP, None),
        P(EP_TP, None),
        P(EP, None, "tp"),
        P(EP, None, "tp"),
        P(EP, "tp", None),
    )
    return jax.shard_map(
        body,
        mesh=split,
        in_specs=placed,
        out_specs=(P(EP_TP, None), P(EP_TP, None)),
        check_vma=False,
    )
```

profile of v0, /device:TPU:1, one launch (start us, length us, event | category | flops | bytes accessed | tf_op | source)
XLA Modules:
  0.0 368.3 jit_solution(15211746906782629320)
XLA Ops:
  7.2 12.6 %all-gather = bf16[768,1,128]{2,0,1:T(8,128)(2,1)} all-gather(bf16[192,1,128]{2,0,1:T(8,128)(2,1)} %param.18), channel_id=2, replica_groups=mesh['ep_0'=8,'ep_1'=4,'ep_2'=2,'tp'=4] {'ep_1'}, dimensions={0}, use_global_device_ids=true | all-gather | bytes 245760 | tf_op jit(solution)/shard_map/all_gather | solution.py:25
  19.9 10.2 %all-gather.1 = bf16[768,1,128]{2,0,1:T(8,128)(2,1)} all-gather(bf16[192,1,128]{2,0,1:T(8,128)(2,1)} %param.19), channel_id=3, replica_groups=mesh['ep_0'=8,'ep_1'=4,'ep_2'=2,'tp'=4] {'ep_1'}, dimensions={0}, use_global_device_ids=true | all-gather | bytes 245760 | tf_op jit(solution)/shard_map/all_gather | solution.py:25
  34.3 1.5 convolution_convert_fusion.1
  36.3 47.2 %all_to_all.34 = bf16[64,4,2048]{2,1,0:T(4,128)(2,1)S(1)} all-to-all(bf16[64,4,2048]{2,1,0:T(4,128)(2,1)S(1)} %all_to_all.23), channel_id=1, replica_groups=mesh['ep_0'=8,'ep_1'=4,'ep_2'=2,'tp'=4] {'ep_0','ep_1','ep_2'}, dimensions={0} | all-to-all | bytes 2097152 | tf_op jit(solution)/shard_map/all_to_all | solution.py:171
  85.2 23.4 %all-gather.12.cloned.1.call-done = bf16[32,192,1,128]{3,1,2,0:T(8,128)(2,1)} async-done(((bf16[4,192,1,128]{3,1,2,0:T(8,128)(2,1)}), bf16[32,192,1,128]{3,1,2,0:T(8,128)(2,1)}) %all-gather.12.cloned.1.call-update) | async-done | bytes 1572880 | tf_op jit(solution)/shard_map/all_gather | solution.py:25
  108.7 54.8 %all-gather.16.cloned.1.call-done = bf16[1024,2048]{1,0:T(8,128)(2,1)} async-done(((bf16[256,2048]{1,0:T(8,128)(2,1)}), bf16[1024,2048]{1,0:T(8,128)(2,1)}) %all-gather.16.cloned.1.call-update) | async-done | bytes 4194320 | tf_op jit(solution)/shard_map/all_gather | solution.py:172
  163.5 7.5 %fusion.16 = f32[1024,896]{1,0:T(8,128)S(1)} fusion(bf16[1024,2048]{1,0:T(8,128)(2,1)} %all-gather.16.cloned.1.call-done, bf16[1,2048,896]{2,1,0:T(8,128)(2,1)} %param.28), kind=kOutput, calls=%fused_computation.26 | convolution fusion | flops 3758096384 | bytes 11534336 | tf_op jit(solution)/shard_map/dot_general | solution.py:174
  171.0 4.7 %multiply_convert_fusion = bf16[1024,896]{1,0:T(8,128)(2,1)S(1)} fusion(f32[1024,896]{1,0:T(8,128)S(1)} %fusion.16, bf16[1024,2048]{1,0:T(8,128)(2,1)S(1)} %copy-done.5, bf16[1,2048,896]{2,1,0:T(8,128)(2,1)S(1)} %copy-done.6), kind=kOutput, calls=%fused_computation.30 | convolution fusion | flops 3763601408 | bytes 13369344 | tf_op jit(solution)/shard_map/dot_general | solution.py:173
  175.8 6.1 %convolution_convert_fusion = bf16[1024,2048]{1,0:T(8,128)(2,1)} fusion(bf16[1024,896]{1,0:T(8,128)(2,1)S(1)} %multiply_convert_fusion, bf16[1,896,2048]{2,1,0:T(8,128)(2,1)S(1)} %copy-done.7), kind=kOutput, calls=%fused_computation.24 | convolution fusion | flops 3760193536 | bytes 9699328 | tf_op jit(solution)/shard_map/dot_general | solution.py:182
  181.9 5.1 %all-to-all-start.2 = ((bf16[4,256,2048]{2,1,0:T(8,128)(2,1)}), bf16[4,256,2048]{2,1,0:T(8,128)(2,1)}, u32[]{:S(2)}, u32[]{:S(2)}) async-start(bf16[4,256,2048]{2,1,0:T(8,128)(2,1)} %bitcast.121), calls=%async_computation.2 | async-start | bytes 8388608 | tf_op jit(solution)/shard_map/all_to_all | solution.py:43
  187.2 11.2 %copy.79 = bf16[8,4,2,192,1,128]{3,2,1,0,5,4:T(2,128)(2,1)} copy(bf16[8,4,2,192,1,128]{5,3,1,0,2,4:T(8,128)(2,1)} %bitcast.122) | data formatting | bytes 6291456 | tf_op jit(solution)/shard_map/transpose | solution.py:29
  198.4 9.9 %reshape_reshape_reshape.3 = bf16[12288,1,2,64]{0,3,2,1:T(8,128)(2,1)} reshape(bf16[8,4,2,192,1,128]{3,2,1,0,5,4:T(2,128)(2,1)} %copy.79) | data formatting | bytes 6291456 | tf_op jit(solution)/shard_map/reshape;reshape;reshape | solution.py:111
  208.4 3.9 %copy.81 = bf16[8,4,2,192,1,128]{5,3,2,1,0,4:T(8,128)(2,1)} copy(bf16[8,4,2,192,1,128]{5,3,1,0,2,4:T(8,128)(2,1)} %bitcast.124) | data formatting | bytes 6291456 | tf_op jit(solution)/shard_map/transpose | solution.py:29
  212.3 24.4 %while.17 = (s32[]{:T(128)}, f32[1,2,2,192]{3,1,2,0:T(2,128)S(1)}, f32[1,2,2,192]{3,1,2,0:T(2,128)S(1)}, f32[1,2,2,192,128]{4,3,2,1,0:T(8,128)S(1)}, s32[192]{0:...) while((s32[]{:T(128)}, f32[1,2,2,192]{3,1,2,0:T(2,128)S(1)}, ...), condition=%wide.region_5.6_spmd, body=%wide.region_0.5_spmd.sunk | while | flops 232147968 | bytes 8857645 | solution.py:131
  213.6 4.3 %conditional.2 = ((f32[1,2,2,192]{3,1,2,0:T(2,128)S(1)}, f32[1,2,2,192]{3,1,2,0:T(2,128)S(1)}, f32[1,2,2,192,128]{4,3,2,1,0:T(8,128)S(1)})) conditional(s32[]{:T(128)} %convert_element_type.91, (f32[1,2,2,192]{3,1,2,0:T(2,128)S(1)}, f32[1,2,2,192]{3,1,2,0:T(2,128)S(1)}, f32[1,2,2,192,128]{4,3,2,1,0:T(8,128)S(1)}) %tuple.61, (s32[]{:T(128)}, ...), branch_computations={%region_1.0_spmd, %region_2.4_spmd} | conditional | flops 232147968 | bytes 8857422 | solution.py:128
  213.8 1.6 fusion
  216.3 1.5 fusion.3
  237.3 1.3 convolution_convert_fusion.2
  238.6 4.0 %all-to-all-start = ((bf16[4,48,2048]{2,1,0:T(8,128)(2,1)}), bf16[4,48,2048]{2,1,0:T(8,128)(2,1)S(1)}, u32[]{:S(2)}, u32[]{:S(2)}) async-start(bf16[4,48,2048]{2,1,0:T(8,128)(2,1)} %bitcast.30), calls=%async_computation | async-start | bytes 1572864 | tf_op jit(solution)/shard_map/all_to_all | solution.py:43
  242.6 3.1 reduce_sum.78
  246.9 6.6 %all-to-all-done = bf16[4,48,2048]{2,1,0:T(8,128)(2,1)S(1)} async-done(((bf16[4,48,2048]{2,1,0:T(8,128)(2,1)}), bf16[4,48,2048]{2,1,0:T(8,128)(2,1)S(1)}, u32[]{:S(2)}, u32[]{:S(2)}) %all-to-all-start) | async-done | bytes 786464 | tf_op jit(solution)/shard_map/all_to_all | solution.py:43
  253.5 74.0 %all-to-all-start.3 = ((bf16[64,4,2048]{2,1,0:T(4,128)(2,1)}), bf16[64,4,2048]{2,1,0:T(4,128)(2,1)S(1)}, u32[]{:S(2)}, u32[]{:S(2)}) async-start(bf16[64,4,2048]{2,1,0:T(4,128)(2,1)} %all_to_all.27), calls=%async_computation.3 | async-start | bytes 2097152 | tf_op jit(solution)/shard_map/all_to_all | solution.py:188
  328.8 26.8 %all-to-all-done.3 = bf16[64,4,2048]{2,1,0:T(4,128)(2,1)S(1)} async-done(((bf16[64,4,2048]{2,1,0:T(4,128)(2,1)}), bf16[64,4,2048]{2,1,0:T(4,128)(2,1)S(1)}, u32[]{:S(2)}, u32[]{:S(2)}) %all-to-all-start.3) | async-done | bytes 1048608 | tf_op jit(solution)/shard_map/all_to_all | solution.py:188
  357.6 4.2 %multiply_reduce_fusion = bf16[96,2048]{1,0:T(8,128)(2,1)} fusion(bf16[96,2,2048]{2,1,0:T(2,128)(2,1)S(1)} %reshape.217, pred[96,2]{1,0:T(8,128)(4,1)S(1)} %copy.90, f32[96,2]{1,0:T(8,128)S(1)} %copy.85), kind=kLoop, calls=%fused_computation.33 | loop fusion | flops 1376256 | bytes 1180608 | tf_op jit(solution)/shard_map/reduce_sum | solution.py:190
  (108 shorter events, 22.3 us)
Async XLA Ops:
  7.2 230.1 %copy-start = (bf16[2,128,2048]{2,1,0:T(8,128)(2,1)S(1)}, bf16[2,128,2048]{2,1,0:T(8,128)(2,1)}, u32[]{:S(2)}) copy-start(bf16[2,128,2048]{2,1,0:T(8,128)(2,1)} %param.22) | copy-start | bytes 3145732
  7.2 77.5 %all-gather.8.cloned.1.call-start = ((), (), s32[]{:S(2)}) async-start(), calls=%async_computation.4 | async-start | bytes 1769472 | tf_op jit(solution)/shard_map/all_gather | solution.py:25
  19.9 88.8 %all-gather.12.cloned.1.call-start = ((), (), s32[]{:S(2)}) async-start(), calls=%async_computation.6 | async-start | bytes 1769472 | tf_op jit(solution)/shard_map/all_gather | solution.py:25
  30.1 133.4 %all-gather.16.cloned.1.call-start = ((), (), s32[]{:S(2)}) async-start(), calls=%async_computation.8 | async-start | bytes 5242880 | tf_op jit(solution)/shard_map/all_gather | solution.py:172
  84.6 102.6 %all-gather.10.cloned.1.call-start = ((), (), s32[]{:S(2)}) async-start(), calls=%async_computation.5 | async-start | bytes 4718592 | tf_op jit(solution)/shard_map/all_gather | solution.py:25
  85.2 123.2 %all-gather.14.cloned.1.call-start = ((), (), s32[]{:S(2)}) async-start(), calls=%async_computation.7 | async-start | bytes 4718592 | tf_op jit(solution)/shard_map/all_gather | solution.py:25
  163.5 7.5 %copy-start.5 = (bf16[1024,2048]{1,0:T(8,128)(2,1)S(1)}, bf16[1024,2048]{1,0:T(8,128)(2,1)}, u32[]{:S(2)}) copy-start(bf16[1024,2048]{1,0:T(8,128)(2,1)} %all-gather.16.cloned.1.call-done) | copy-start | bytes 12582916
  163.5 7.5 %copy-start.6 = (bf16[1,2048,896]{2,1,0:T(8,128)(2,1)S(1)}, bf16[1,2048,896]{2,1,0:T(8,128)(2,1)}, u32[]{:S(2)}) copy-start(bf16[1,2048,896]{2,1,0:T(8,128)(2,1)} %param.27) | copy-start | bytes 11010052
  171.0 4.8 %copy-start.7 = (bf16[1,896,2048]{2,1,0:T(8,128)(2,1)S(1)}, bf16[1,896,2048]{2,1,0:T(8,128)(2,1)}, u32[]{:S(2)}) copy-start(bf16[1,896,2048]{2,1,0:T(8,128)(2,1)} %param.29) | copy-start | bytes 11010052
  181.9 5.2 %copy-start.1 = (bf16[192,2,128]{2,1,0:T(2,128)(2,1)S(1)}, bf16[192,2,128]{2,1,0:T(2,128)(2,1)}, u32[]{:S(2)}) copy-start(bf16[192,2,128]{2,1,0:T(2,128)(2,1)} %param.17) | copy-start | bytes 294916
  181.9 56.7 %all-to-all-start.2 = ((bf16[4,256,2048]{2,1,0:T(8,128)(2,1)}), bf16[4,256,2048]{2,1,0:T(8,128)(2,1)}, u32[]{:S(2)}, u32[]{:S(2)}) async-start(bf16[4,256,2048]{2,1,0:T(8,128)(2,1)} %bitcast.121), calls=%async_computation.2 | async-start | bytes 8388608 | tf_op jit(solution)/shard_map/all_to_all | solution.py:43
  212.3 24.4 %copy-start.4 = (f32[2]{0:T(128)S(1)}, f32[2]{0:T(128)}, u32[]{:S(2)}) copy-start(f32[2]{0:T(128)} %param.20) | copy-start | bytes 28
  212.3 24.7 %copy-start.3 = (f32[128]{0:T(128)S(1)}, f32[128]{0:T(128)}, u32[]{:S(2)}) copy-start(f32[128]{0:T(128)} %param.21) | copy-start | bytes 1540
  238.6 14.9 %all-to-all-start = ((bf16[4,48,2048]{2,1,0:T(8,128)(2,1)}), bf16[4,48,2048]{2,1,0:T(8,128)(2,1)S(1)}, u32[]{:S(2)}, u32[]{:S(2)}) async-start(bf16[4,48,2048]{2,1,0:T(8,128)(2,1)} %bitcast.30), calls=%async_computation | async-start | bytes 1572864 | tf_op jit(solution)/shard_map/all_to_all | solution.py:43
  245.7 82.2 %copy-start.2 = (f32[96,2]{0,1:T(2,128)S(1)}, f32[96,2]{0,1:T(2,128)}, u32[]{:S(2)}) copy-start(f32[96,2]{0,1:T(2,128)} %param.26) | copy-start | bytes 2308
  253.5 102.2 %all-to-all-start.3 = ((bf16[64,4,2048]{2,1,0:T(4,128)(2,1)}), bf16[64,4,2048]{2,1,0:T(4,128)(2,1)S(1)}, u32[]{:S(2)}, u32[]{:S(2)}) async-start(bf16[64,4,2048]{2,1,0:T(4,128)(2,1)} %all_to_all.27), calls=%async_computation.3 | async-start | bytes 2097152 | tf_op jit(solution)/shard_map/all_to_all | solution.py:188
Sparse Core Ops, SparseCore 0:
  20.0 43.5 all-gather.7
  65.3 43.2 all-gather.11
  110.5 52.9 all-gather.15
  165.2 18.7 all-gather.9
  185.6 18.7 all-gather.13
where the time goes:
time: 370 us; the launch traced here: 368 us
  waiting for transfers between devices  112 us (30%)
  starting transfers between devices  83.3 us (23%)
  blocking collectives  70 us (19%)
  local copies, waits for them, and re-layouts  41.2 us (11%)
  matrix products  24.3 us (7%)
  between operations  14.1 us (4%)
  other arithmetic  12.4 us (3%)
  loops' own time  10.7 us (3%)
    all_to_all x1, starting transfers between devices, body(): lax.all_to_all(expert_out, EP, split_axis=0, concat_axis=0, tiled=True)  74 us
    all_gather x1, waiting for transfers between devices, body(): inputs = lax.all_gather(received, 'tp', axis=0, tiled=True)  54.8 us
    all_to_all x1, blocking collectives, body(): lax.all_to_all(outbound, EP, split_axis=0, concat_axis=0, tiled=True)  47.2 us
    all_to_all x1, waiting for transfers between devices, body(): lax.all_to_all(expert_out, EP, split_axis=0, concat_axis=0, tiled=True)  26.8 us
    all_gather x4, waiting for transfers between devices, gather_in_order(): tiles = lax.all_gather(tiles, axes[k], axis=0, tiled=True)  23.5 us
    all_gather x2, blocking collectives, gather_in_order(): tiles = lax.all_gather(tiles, axes[k], axis=0, tiled=True)  22.8 us
    transpose x2, local copies, waits for them, and re-layouts, gather_in_order(): tiles.transpose(*turned, *range(len(order), tiles.ndim))  15.1 us
    another operation x1, loops' own time, body(): folded = lax.fori_loop(0, length // span, sweep, initial)  10.4 us
  transfers between devices with their start and end apart: 8, of which 4 were waited for; matrix products, arithmetic and copies ran while one was open for 19% of the time, Pallas kernels for 0%

commit v1 on v0

v1 whole, which is shorter than its diff:
```python
import functools

import jax
import jax.numpy as jnp
from jax import lax
from jax.experimental import pallas as pl
from jax.experimental.pallas import tpu as pltpu
from jax.sharding import Mesh
from jax.sharding import PartitionSpec as P

EP = ("ep_0", "ep_1", "ep_2")
EP_TP = ("ep_0", "ep_1", "ep_2", "tp")
MESH = pl.DeviceIdType.MESH

NZ, NY, NC, NX = 8, 4, 2, 4
CHUNKS = NY
BLOCKS = NZ * NC
CAP = 4
QUARTERS = 4
GROUP = BLOCKS * CAP
NEG_LARGE = -1e30
F32 = jnp.float32
BF16 = jnp.bfloat16


def dz_order():
    return (1, 7, 2, 6, 3, 5, 4, 0)


def kernel(
    outbound,
    q_ref,
    k_ref,
    v_ref,
    ow_ref,
    comb_ref,
    mix_ref,
    gain_ref,
    gw_hbm,
    uw_hbm,
    dw_hbm,
    attn_o,
    moe_o,
    gw,
    uw,
    dw,
    kbuf,
    vbuf,
    perm,
    perm_t,
    arr,
    xb,
    hid,
    part,
    opp,
    fin,
    back,
    ret,
    rows_ref,
    m_ref,
    l_ref,
    acc_ref,
    att_ref,
    ap,
    ar,
    w_sem,
    kv_own,
    kv_send,
    kv_recv,
    a_send,
    a_recv,
    x_send,
    x_recv,
    f_send,
    f_recv,
    s1_send,
    s1_recv,
    s2_send,
    fin_recv,
    b_send,
    r_recv,
    at_send,
    at_recv,
):
    z = lax.axis_index("ep_0")
    y = lax.axis_index("ep_1")
    c = lax.axis_index("ep_2")
    x = lax.axis_index("tp")
    me = z * (NY * NC) + y * NC + c
    right = {"tp": lax.rem(x + 1, NX)}
    left = {"tp": lax.rem(x + NX - 1, NX)}
    y_up = {"ep_1": lax.rem(y + 1, NY)}
    y_down = {"ep_1": lax.rem(y + NY - 1, NY)}
    ym1 = lax.rem(y + NY - 1, NY)
    yp1 = lax.rem(y + 1, NY)
    partner = {"ep_2": 1 - c}

    def rcopy(src, dst, ssem, rsem, dev):
        return pltpu.make_async_remote_copy(
            src_ref=src, dst_ref=dst, send_sem=ssem, recv_sem=rsem, device_id=dev, device_id_type=MESH
        )

    weights = [
        pltpu.make_async_copy(s, d, w_sem.at[i]) for i, (s, d) in enumerate(((gw_hbm, gw), (uw_hbm, uw), (dw_hbm, dw)))
    ]
    for copy in weights:
        copy.start()

    def send_rows(g, carry):
        for dz in dz_order():
            for dc in range(NC):
                i = dz * NC + dc

                def go():
                    dev = {
                        "ep_0": lax.rem(z + dz, NZ),
                        "ep_1": lax.rem(y + g, NY),
                        "ep_2": (1 - c) if dc else c,
                    }
                    rcopy(outbound.at[g, i], arr.at[g, i], a_send.at[0], a_recv.at[g], dev).start()

                if i == 0:
                    pl.when(g > 0)(go)
                else:
                    go()
        return carry

    lax.fori_loop(0, CHUNKS, send_rows, 0)
    pltpu.make_async_copy(outbound.at[0, 0], arr.at[0, 0], a_recv.at[0]).start()

    kv = ((k_ref, kbuf, 0), (v_ref, vbuf, 1))
    kv_z = []
    for ref, buf, j in kv:
        pltpu.make_async_copy(ref, buf.at[z, y, c], kv_own.at[j]).start()
        for dz in (1, 7, 2, 6, 3, 5, 4):
            copy = rcopy(ref, buf.at[z, y, c], kv_send.at[0, j], kv_recv.at[0, j], {"ep_0": lax.rem(z + dz, NZ)})
            copy.start()

    def kv_y():
        for ref, buf, j in kv:
            pltpu.make_async_copy(ref, buf.at[z, y, c], kv_own.at[j]).wait()
            pltpu.make_async_copy(
                buf.at[pl.ds(0, NZ - 1), y, c], buf.at[pl.ds(0, NZ - 1), y, c], kv_recv.at[0, j]
            ).wait()
            rcopy(buf.at[:, y, c], buf.at[:, y, c], kv_send.at[1, j], kv_recv.at[1, j], y_up).start()
            rcopy(buf.at[:, y, c], buf.at[:, y, c], kv_send.at[2, j], kv_recv.at[2, j], y_down).start()

    half = NZ // 2

    def kv_y2():
        for ref, buf, j in kv:
            rcopy(buf.at[:, ym1, c], buf.at[:, ym1, c], kv_send.at[1, j], kv_recv.at[1, j], y_up).wait_recv()
            lo = buf.at[pl.ds(0, half), ym1, c]
            rcopy(lo, lo, kv_send.at[3, j], kv_recv.at[3, j], y_up).start()
            rcopy(buf.at[:, yp1, c], buf.at[:, yp1, c], kv_send.at[2, j], kv_recv.at[2, j], y_down).wait_recv()
            hi = buf.at[pl.ds(half, half), yp1, c]
            rcopy(hi, hi, kv_send.at[4, j], kv_recv.at[4, j], y_down).start()

    def kv_core():
        yo = lax.rem(y + 2, NY)
        for ref, buf, j in kv:
            lo = buf.at[pl.ds(0, half), yo, c]
            rcopy(lo, lo, kv_send.at[3, j], kv_recv.at[3, j], y_up).wait_recv()
            hi = buf.at[pl.ds(half, half), yo, c]
            rcopy(hi, hi, kv_send.at[4, j], kv_recv.at[4, j], y_down).wait_recv()
            rcopy(buf.at[:, :, c], buf.at[:, :, c], kv_send.at[5, j], kv_recv.at[5, j], partner).start()

    size = BLOCKS * QUARTERS * CAP
    r_io = lax.broadcasted_iota(jnp.int32, (size, size), 0)
    c_io = lax.broadcasted_iota(jnp.int32, (size, size), 1)

    def packed_place(r):
        return (r % GROUP) // CAP * (QUARTERS * CAP) + r // GROUP * CAP + r % CAP

    perm[...] = (packed_place(r_io) == c_io).astype(BF16)
    perm_t[...] = (packed_place(c_io) == r_io).astype(BF16)
    width = outbound.shape[-1]

    def relayout_in(src, g, store):
        tile = src[g].reshape(size, width)
        turned = jnp.dot(perm[...], tile, preferred_element_type=F32).astype(BF16)
        for kq in range(QUARTERS):
            store(kq, turned[kq * GROUP : (kq + 1) * GROUP])

    def gather_first(g):
        pltpu.make_async_copy(arr.at[g], arr.at[g], a_recv.at[g]).wait()

        def store(kq, value):
            xb[g, 0, :, kq * width : (kq + 1) * width] = value

        relayout_in(arr, g, store)
        rcopy(xb.at[g, 0], xb.at[g, 1], x_send.at[0, g], x_recv.at[0, g], right).start()
        rcopy(xb.at[g, 0], xb.at[g, 2], x_send.at[1, g], x_recv.at[1, g], left).start()

    top, low = pl.ds(0, GROUP // 2), pl.ds(GROUP // 2, GROUP // 2)

    def gather_second(g):
        rcopy(xb.at[g, 0], xb.at[g, 1], x_send.at[0, g], x_recv.at[0, g], right).wait_recv()
        rcopy(xb.at[g, 1, top], xb.at[g, 3, top], f_send.at[0, g], f_recv.at[0, g], right).start()
        rcopy(xb.at[g, 0], xb.at[g, 2], x_send.at[1, g], x_recv.at[1, g], left).wait_recv()
        rcopy(xb.at[g, 2, low], xb.at[g, 3, low], f_send.at[1, g], f_recv.at[1, g], left).start()

    ffe = gw.shape[1]
    model = gw.shape[0]
    rows = NX * GROUP

    def experts(g):
        rcopy(xb.at[g, 1, top], xb.at[g, 3, top], f_send.at[0, g], f_recv.at[0, g], right).wait_recv()
        rcopy(xb.at[g, 2, low], xb.at[g, 3, low], f_send.at[1, g], f_recv.at[1, g], left).wait_recv()

        @pl.when(g == 0)
        def _():
            for copy in weights:
                copy.wait()

        inputs = xb[g].reshape(rows, model)
        for n in range(0, ffe, 256):
            w = min(256, ffe - n)
            gate = jnp.dot(inputs, gw[:, n : n + w], preferred_element_type=F32)
            up = jnp.dot(inputs, uw[:, n : n + w], preferred_element_type=F32)
            hid[:, n : n + w] = (gate / (1.0 + jnp.exp(-gate)) * up).astype(BF16)
        hidden = hid[...]
        for n in range(0, model, 256):
            part[g, :, :, n : n + 256] = (
                jnp.dot(hidden, dw[:, n : n + 256], preferred_element_type=F32).astype(BF16).reshape(NX, GROUP, 256)
            )
        rcopy(part.at[g, 3, top], opp.at[g, 0], s1_send.at[0, g], s1_recv.at[0, g], right).start()
        rcopy(part.at[g, 3, low], opp.at[g, 1], s1_send.at[1, g], s1_recv.at[1, g], left).start()
        rcopy(part.at[g, 2, low], fin.at[g, 0, low], s2_send.at[0, g], fin_recv.at[0, g], right).start()
        rcopy(part.at[g, 1, top], fin.at[g, 1, top], s2_send.at[1, g], fin_recv.at[1, g], left).start()

    def sum_second(g):
        rcopy(part.at[g, 3, top], opp.at[g, 0], s1_send.at[0, g], s1_recv.at[0, g], right).wait_recv()
        part[g, 2, : GROUP // 2] = (part[g, 2, : GROUP // 2].astype(F32) + opp[g, 0].astype(F32)).astype(BF16)
        rcopy(part.at[g, 2, top], fin.at[g, 0, top], s2_send.at[2, g], fin_recv.at[2, g], right).start()
        rcopy(part.at[g, 3, low], opp.at[g, 1], s1_send.at[1, g], s1_recv.at[1, g], left).wait_recv()
        part[g, 1, GROUP // 2 :] = (part[g, 1, GROUP // 2 :].astype(F32) + opp[g, 1].astype(F32)).astype(BF16)
        rcopy(part.at[g, 1, low], fin.at[g, 1, low], s2_send.at[3, g], fin_recv.at[3, g], left).start()

    def sum_last(g):
        rcopy(part.at[g, 2, low], fin.at[g, 0, low], s2_send.at[0, g], fin_recv.at[0, g], right).wait_recv()
        rcopy(part.at[g, 1, top], fin.at[g, 1, top], s2_send.at[1, g], fin_recv.at[1, g], left).wait_recv()
        rcopy(part.at[g, 2, top], fin.at[g, 0, top], s2_send.at[2, g], fin_recv.at[2, g], right).wait_recv()
        rcopy(part.at[g, 1, low], fin.at[g, 1, low], s2_send.at[3, g], fin_recv.at[3, g], left).wait_recv()
        total = (part[g, 0].astype(F32) + fin[g, 0].astype(F32) + fin[g, 1].astype(F32)).astype(BF16)
        tall = jnp.concatenate([total[:, kq * width : (kq + 1) * width] for kq in range(QUARTERS)], axis=0)
        back[g] = (
            jnp.dot(perm_t[...], tall, preferred_element_type=F32).astype(BF16).reshape(BLOCKS, QUARTERS * CAP, width)
        )
        for dz in dz_order():
            for dc in range(NC):
                i = dz * NC + dc

                def go():
                    dev = {
                        "ep_0": lax.rem(z + NZ - dz, NZ),
                        "ep_1": lax.rem(y + NY - g, NY),
                        "ep_2": (1 - c) if dc else c,
                    }
                    rcopy(back.at[g, i], ret.at[g, i], b_send.at[0], r_recv.at[g], dev).start()

                if i == 0:
                    pl.when(g > 0)(go)

                    @pl.when(g == 0)
                    def _():
                        pltpu.make_async_copy(back.at[0, 0], ret.at[0, 0], r_recv.at[0]).start()

                else:
                    go()

    ta = q_ref.shape[1]
    heads = q_ref.shape[0] // 2
    span = 2 * NC * ta

    def attend():
        for ref, buf, j in kv:
            rcopy(
                buf.at[:, :, 1 - c], buf.at[:, :, 1 - c], kv_send.at[5, j], kv_recv.at[5, j], partner
            ).wait_recv()
        m_ref[...] = jnp.full(m_ref.shape, NEG_LARGE, F32)
        l_ref[...] = jnp.zeros(l_ref.shape, F32)
        acc_ref[...] = jnp.zeros(acc_ref.shape, F32)

        def chunk(t, masked):
            zz = t // 2
            yh = t % 2
            kc = kbuf[zz, pl.ds(yh * 2, 2)].reshape(span, kbuf.shape[-1])
            vc = vbuf[zz, pl.ds(yh * 2, 2)].reshape(span, vbuf.shape[-1])
            for r in range(2 * heads):
                s = lax.dot_general(q_ref[r], kc, (((1,), (1,)), ((), ())), preferred_element_type=F32)
                if masked:
                    kpos = t * span + lax.broadcasted_iota(jnp.int32, s.shape, 1)
                    qpos = me * ta + lax.broadcasted_iota(jnp.int32, s.shape, 0)
                    s = jnp.where(kpos <= qpos, s, NEG_LARGE)
                old = m_ref[r][:, :1]
                new = jnp.maximum(old, jnp.max(s, axis=1, keepdims=True))
                p = jnp.exp(s - new)
                scale = jnp.exp(old - new)
                l_ref[r] = jnp.broadcast_to(
                    l_ref[r][:, :1] * scale + jnp.sum(p, axis=1, keepdims=True), l_ref.shape[1:]
                )
                m_ref[r] = jnp.broadcast_to(new, m_ref.shape[1:])
                acc_ref[r] = acc_ref[r] * scale + jnp.dot(p.astype(BF16), vc, preferred_element_type=F32)

        last = me // (2 * NC)

        def step(t, carry):
            chunk(t, False)
            return carry

        lax.fori_loop(0, last, step, 0)
        chunk(last, True)
        for h in range(heads):
            blended = acc_ref[h] / l_ref[h] - mix_ref[h] * (acc_ref[heads + h] / l_ref[heads + h])
            normed = (
                blended * lax.rsqrt(jnp.mean(blended * blended, axis=1, keepdims=True) + 1e-05) * gain_ref[...]
            ).astype(BF16)
            att_ref[:, :, h * 128 : (h + 1) * 128] = normed.reshape(NX, ta // NX, 128)
        for r in range(NX):
            j = lax.rem(x + r, NX)
            ap[r] = jnp.dot(att_ref[j], ow_ref[...], preferred_element_type=F32).astype(BF16)
            if r:
                rcopy(ap.at[r], ar.at[r - 1], at_send.at[r - 1], at_recv.at[r - 1], {"tp": j}).start()

    def main(s, carry):
        @pl.when((s >= 4) & (s < CHUNKS + 4))
        def _():
            sum_last(s - 4)

        @pl.when((s >= 3) & (s < CHUNKS + 3))
        def _():
            sum_second(s - 3)

        @pl.when(s < CHUNKS)
        def _():
            gather_first(s)

        @pl.when((s >= 1) & (s < CHUNKS + 1))
        def _():
            gather_second(s - 1)

        pl.when(s == 1)(kv_y)
        pl.when(s == 2)(kv_y2)
        pl.when(s == 3)(kv_core)

        @pl.when((s >= 2) & (s < CHUNKS + 2))
        def _():
            experts(s - 2)

        pl.when(s == CHUNKS + 1)(attend)
        return carry

    lax.fori_loop(0, CHUNKS + 4, main, 0)

    for r in range(1, NX):
        rcopy(ap.at[r], ar.at[r - 1], at_send.at[r - 1], at_recv.at[r - 1], right).wait_recv()
    total = ap[0].astype(F32)
    for r in range(1, NX):
        total = total + ar[r - 1].astype(F32)
    attn_o[...] = total.astype(BF16)

    def collect(g, carry):
        pltpu.make_async_copy(ret.at[g], ret.at[g], r_recv.at[g]).wait()

        def store(kq, value):
            rows_ref[pl.ds(pl.multiple_of(g * GROUP, GROUP), GROUP), kq * width : (kq + 1) * width] = value

        relayout_in(ret, g, store)
        return carry

    lax.fori_loop(0, CHUNKS, collect, 0)
    tokens = moe_o.shape[0]
    for kq in range(QUARTERS):
        both = jnp.dot(comb_ref[...], rows_ref[:, kq * width : (kq + 1) * width], preferred_element_type=F32)
        moe_o[:, kq * width : (kq + 1) * width] = (both[:tokens] + both[tokens:]).astype(BF16)

    for g in range(CHUNKS):
        for copy in (
            rcopy(xb.at[g, 0], xb.at[g, 1], x_send.at[0, g], x_recv.at[0, g], right),
            rcopy(xb.at[g, 0], xb.at[g, 2], x_send.at[1, g], x_recv.at[1, g], left),
            rcopy(xb.at[g, 1, top], xb.at[g, 3, top], f_send.at[0, g], f_recv.at[0, g], right),
            rcopy(xb.at[g, 2, low], xb.at[g, 3, low], f_send.at[1, g], f_recv.at[1, g], left),
            rcopy(part.at[g, 3, top], opp.at[g, 0], s1_send.at[0, g], s1_recv.at[0, g], right),
            rcopy(part.at[g, 3, low], opp.at[g, 1], s1_send.at[1, g], s1_recv.at[1, g], left),
            rcopy(part.at[g, 2, low], fin.at[g, 0, low], s2_send.at[0, g], fin_recv.at[0, g], right),
            rcopy(part.at[g, 1, top], fin.at[g, 1, top], s2_send.at[1, g], fin_recv.at[1, g], left),
            rcopy(part.at[g, 2, top], fin.at[g, 0, top], s2_send.at[2, g], fin_recv.at[2, g], right),
            rcopy(part.at[g, 1, low], fin.at[g, 1, low], s2_send.at[3, g], fin_recv.at[3, g], left),
        ):
            copy.wait_send()
    for r in range(1, NX):
        rcopy(ap.at[r], ar.at[r - 1], at_send.at[r - 1], at_recv.at[r - 1], right).wait_send()
    for ref, buf, j in kv:
        seven = buf.at[pl.ds(0, NZ - 1), y, c]
        rcopy(seven, seven, kv_send.at[0, j], kv_recv.at[0, j], y_up).wait_send()
        for n in (1, 2):
            rcopy(buf.at[:, y, c], buf.at[:, y, c], kv_send.at[n, j], kv_recv.at[n, j], y_up).wait_send()
        for n in (3, 4):
            lo = buf.at[pl.ds(0, half), y, c]
            rcopy(lo, lo, kv_send.at[n, j], kv_recv.at[n, j], y_up).wait_send()
        rcopy(buf.at[:, :, c], buf.at[:, :, c], kv_send.at[5, j], kv_recv.at[5, j], partner).wait_send()
    for sem, buf in ((a_send, outbound), (b_send, back)):
        for g in range(CHUNKS):
            blocks = buf.at[g, pl.ds(1, BLOCKS - 1)] if g == 0 else buf.at[g]
            rcopy(blocks, blocks, sem.at[0], r_recv.at[g], right).wait_send()


def body(
    queries,
    keys,
    values,
    mix_scale,
    head_gain,
    out_weight,
    moe_input,
    norm_gain,
    routes,
    route_weights,
    gate_weight,
    up_weight,
    down_weight,
):
    ta, heads, qd = queries.shape
    tok, model = moe_input.shape
    ffe = gate_weight.shape[2]
    vd = values.shape[2]
    width = model // QUARTERS
    z = lax.axis_index("ep_0")
    y = lax.axis_index("ep_1")
    c = lax.axis_index("ep_2")

    widened = moe_input.astype(F32)
    normed = (
        widened * lax.rsqrt(jnp.mean(widened * widened, axis=-1, keepdims=True) + 1e-06) * norm_gain
    ).astype(BF16)
    flat = routes.reshape(-1)
    count = flat.shape[0]
    places = jnp.arange(count, dtype=jnp.int32)
    earlier = (flat[:, None] == flat[None, :]) & (places[None, :] < places[:, None])
    rank = jnp.sum(earlier.astype(jnp.int32), axis=1).reshape(routes.shape)
    ez, ey, ec = routes // (NY * NC), (routes // NC) % NY, routes % NC
    offset = ((ey - y) % NY) * BLOCKS + ((ez - z) % NZ) * NC + (ec + c) % NC
    slot = offset * CAP + rank
    slots = NY * BLOCKS * CAP

    r = jnp.arange(slots * QUARTERS, dtype=jnp.int32)
    r_slot = r // (QUARTERS * CAP) * CAP + r % CAP
    r_quarter = (r // CAP) % QUARTERS
    col = jnp.arange(QUARTERS * tok, dtype=jnp.int32)
    col_quarter = col // tok
    col_slot = jnp.tile(slot, (QUARTERS, 1))
    chosen = (r_slot[:, None] == col_slot[None, :, 0]) | (r_slot[:, None] == col_slot[None, :, 1])
    dispatch = (chosen & (r_quarter[:, None] == col_quarter[None, :])).astype(BF16)
    stacked = normed.reshape(tok, QUARTERS, width).transpose(1, 0, 2).reshape(QUARTERS * tok, width)
    outbound = jnp.dot(dispatch, stacked, preferred_element_type=F32).astype(BF16)
    outbound = outbound.reshape(CHUNKS, BLOCKS, QUARTERS * CAP, width)

    places = jnp.arange(slots, dtype=jnp.int32)
    comb = jnp.sum(
        jnp.where(slot[:, :, None] == places[None, None, :], route_weights[:, :, None], 0.0), axis=1
    )
    high = comb.astype(BF16)
    comb = jnp.concatenate([high, (comb - high.astype(F32)).astype(BF16)], axis=0)

    scaled = (queries.astype(F32) * (1.0 / (qd // 2) ** 0.5)).astype(BF16).transpose(1, 0, 2)
    lane = jnp.arange(qd, dtype=jnp.int32)[None, None, :]
    zero = jnp.zeros((), BF16)
    q_all = jnp.concatenate(
        [jnp.where(lane < qd // 2, scaled, zero), jnp.where(lane < qd // 2, zero, scaled)], axis=0
    )

    vmem = pl.BlockSpec(memory_space=pltpu.VMEM)
    hbm = pl.BlockSpec(memory_space=pl.ANY)
    dma = pltpu.SemaphoreType.DMA
    size = BLOCKS * QUARTERS * CAP
    attn_out, moe_out = pl.pallas_call(
        kernel,
        out_shape=(
            jax.ShapeDtypeStruct((ta // NX, model), BF16),
            jax.ShapeDtypeStruct((tok, model), BF16),
        ),
        in_specs=[vmem] * 6 + [pl.BlockSpec(memory_space=pltpu.SMEM), vmem] + [hbm] * 3,
        out_specs=(vmem, vmem),
        scratch_shapes=[
            pltpu.VMEM((model, ffe), BF16),
            pltpu.VMEM((model, ffe), BF16),
            pltpu.VMEM((ffe, model), BF16),
            pltpu.VMEM((NZ, NY, NC, ta, qd), BF16),
            pltpu.VMEM((NZ, NY, NC, ta, vd), BF16),
            pltpu.VMEM((size, size), BF16),
            pltpu.VMEM((size, size), BF16),
            pltpu.VMEM((CHUNKS, BLOCKS, QUARTERS * CAP, width), BF16),
            pltpu.VMEM((CHUNKS, NX, GROUP, model), BF16),
            pltpu.VMEM((NX * GROUP, ffe), BF16),
            pltpu.VMEM((CHUNKS, NX, GROUP, model), BF16),
            pltpu.VMEM((CHUNKS, 2, GROUP // 2, model), BF16),
            pltpu.VMEM((CHUNKS, 2, GROUP, model), BF16),
            pltpu.VMEM((CHUNKS, BLOCKS, QUARTERS * CAP, width), BF16),
            pltpu.VMEM((CHUNKS, BLOCKS, QUARTERS * CAP, width), BF16),
            pltpu.VMEM((slots, model), BF16),
            pltpu.VMEM((2 * heads, ta, 128), F32),
            pltpu.VMEM((2 * heads, ta, 128), F32),
            pltpu.VMEM((2 * heads, ta, vd), F32),
            pltpu.VMEM((NX, ta // NX, heads * vd), BF16),
            pltpu.VMEM((NX, ta // NX, model), BF16),
            pltpu.VMEM((NX - 1, ta // NX, model), BF16),
            dma((3,)),
            dma((2,)),
            dma((6, 2)),
            dma((6, 2)),
            dma((1,)),
            dma((CHUNKS,)),
            dma((2, CHUNKS)),
            dma((2, CHUNKS)),
            dma((2, CHUNKS)),
            dma((2, CHUNKS)),
            dma((2, CHUNKS)),
            dma((2, CHUNKS)),
            dma((4, CHUNKS)),
            dma((4, CHUNKS)),
            dma((1,)),
            dma((CHUNKS,)),
            dma((NX - 1,)),
            dma((NX - 1,)),
        ],
        compiler_params=pltpu.CompilerParams(has_side_effects=True, vmem_limit_bytes=62 * 1024 * 1024),
    )(
        outbound,
        q_all,
        keys.reshape(ta, qd),
        values.reshape(ta, vd),
        out_weight.reshape(heads * vd, model),
        comb,
        mix_scale,
        head_gain.reshape(1, vd),
        gate_weight[0],
        up_weight[0],
        down_weight[0],
    )
    return (attn_out, moe_out)


def solution(mesh):
    split = Mesh(mesh.devices.reshape(NZ, NY, NC, NX), EP_TP)
    placed = (
        P(EP, "tp", None),
        P(EP, "tp", None),
        P(EP, "tp", None),
        P("tp"),
        P(),
        P("tp", None, None),
        P(EP_TP, None),
        P(),
        P(EP_TP, None),
        P(EP_TP, None),
        P(EP, None, "tp"),
        P(EP, None, "tp"),
        P(EP, "tp", None),
    )
    return jax.shard_map(
        body,
        mesh=split,
        in_specs=placed,
        out_specs=(P(EP_TP, None), P(EP_TP, None)),
        check_vma=False,
    )
```

time: 370 us -> 177 us (0.48)
  Pallas kernels: 0 us -> 163 us
  waiting for transfers between devices: 112 us -> 0 us
  starting transfers between devices: 83.3 us -> 0 us
  blocking collectives: 70 us -> 0 us
  local copies, waits for them, and re-layouts: 41.2 us -> 5.11 us
  matrix products: 24.3 us -> 1.99 us
  between operations: 14.1 us -> 0.73 us
  loops' own time: 10.7 us -> 0 us
  other arithmetic: 12.4 us -> 5.55 us
    pallas_call x0 -> x1, Pallas kernels: none -> 163 us  [body(): pl.pallas_call(kernel, out_shape=(jax.ShapeDtypeStruct((ta // NX, model),...]
    all_to_all x3 -> x0, starting transfers between devices: 83.1 us -> none  [the longest x1 74 us: body(): lax.all_to_all(expert_out, EP, split_axis=0, concat_axis=0, tiled=True)]
    all_gather x5 -> x0, waiting for transfers between devices: 78.3 us -> none  [the longest x1 54.8 us: body(): inputs = lax.all_gather(received, 'tp', axis=0, tiled=True)]
    all_to_all x1 -> x0, blocking collectives: 47.2 us -> none  [body(): lax.all_to_all(outbound, EP, split_axis=0, concat_axis=0, tiled=True)]
    all_to_all x3 -> x0, waiting for transfers between devices: 33.4 us -> none  [the longest x1 26.8 us: body(): lax.all_to_all(expert_out, EP, split_axis=0, concat_axis=0, tiled=True)]
    all_gather x2 -> x0, blocking collectives: 22.8 us -> none  [gather_in_order(): tiles = lax.all_gather(tiles, axes[k], axis=0, tiled=True)]
    dot_general x7 -> x1, matrix products: 24.3 us -> 1.99 us  [body(): jnp.dot(dispatch, stacked, preferred_element_type=F32).astype(BF16)]
    transpose x3 -> x1, local copies, waits for them, and re-layouts: 15.2 us -> 0.07 us  [body(): normed.reshape(tok, QUARTERS, width).transpose(1, 0, 2)]
  transfers between devices with their start and end apart: 8 -> 0, of which waited for: 4 -> 0; matrix products, arithmetic and copies ran while one was open for 19% -> 0% of each run, Pallas kernels for 0% -> 0%
where the time goes in v1:
time: 177 us; the launch traced here: 176 us
  Pallas kernels  163 us (92%)
  other arithmetic  5.55 us (3%)
  local copies, waits for them, and re-layouts  5.11 us (3%)
  matrix products  1.99 us (1%)
    pallas_call x1, Pallas kernels, body(): pl.pallas_call(kernel, out_shape=(jax.ShapeDtypeStruct((ta // NX, model),...  163 us
    unnamed x7, local copies, waits for them, and re-layouts  4.17 us

profile of v1, /device:TPU:1, one launch (start us, length us, event | category | flops | bytes accessed | tf_op | source)
XLA Modules:
  0.0 176.4 jit_solution(5426166102808704524)
XLA Ops:
  0.6 0.0 copy-start
  0.6 0.0 copy-start.1
  0.7 1.2 fusion.9
  1.9 0.7 broadcast_compare_fusion
  2.6 0.1 copy.51
  2.7 0.8 copy.46
  3.5 0.1 eq.81
  3.7 0.2 convert_reduce_fusion
  3.8 0.1 reshape.109
  4.0 0.2 fusion.25
  4.2 0.1 copy.56
  4.2 0.1 tile.10
  4.4 0.8 select_reduce_fusion
  5.2 0.6 pad_maximum_fusion.1.comb_ref
  5.8 0.9 select_bitcast_fusion.1
  6.8 0.7 pad_maximum_fusion.q_ref
  7.5 0.0 copy-done
  7.5 0.2 fusion.11
  7.6 0.3 reshape.110
  7.9 0.1 copy.57
  8.0 2.0 %fusion.6 = bf16[1024,512]{1,0:T(8,128)(2,1)} fusion(bf16[384,512]{1,0:T(8,128)(2,1)S(1)} %bitcast.23, s32[384]{0:T(512)S(1)} %add_select_fusion.10, s32[384]{0:T(512)S(1)} %get-tuple-element.3, s32[384]{0:T(512)S(1)} %get-tuple-element.2, s32[1024]{0:T(1024)S(1)} %get-tuple-element.8, s32[1024]{0:T(1024)S(1)} %get-tuple-element.9), kind=kOutput, calls=%fused_computation.6 | convolution fusion | flops 405143552 | bytes 1454592 | tf_op jit(solution)/shard_map/dot_general | solution.py:456
  10.0 163.0 %shard_map.140 = (bf16[48,2048]{1,0:T(8,128)(2,1)}, bf16[96,2048]{1,0:T(8,128)(2,1)}) custom-call(bf16[4,16,16,512]{3,2,1,0:T(8,128)(2,1)} %bitcast.22, bf16[4,192,128]{2,1,0:T(8,128)(2,1)} %pad_maximum_fusion.q_ref, bf16[192,128]{1,0:T(8,128)(2,1)} %bitcast.24, bf16[192,128]{1,0:T(8,128)(2,1)} %bitcast.25, bf16[256,2048]{1,0:T(8,128)(2,1)} %bitcast.21, ...), custom_call_target="tpu_custom_call" | custom-call | tf_op jit(solution)/shard_map/pallas_call | solution.py:477
  173.0 1.6 copy.68
  174.6 1.8 %copy.69 = bf16[96,2048]{1,0:T(8,128)(2,1)} copy(bf16[96,2048]{1,0:T(8,128)(2,1)} %get-tuple-element.13) | data formatting | bytes 786432
  (8 shorter events, 0.1 us)
Async XLA Ops:
  0.6 6.8 %copy-start = (bf16[96,2048]{1,0:T(8,128)(2,1)S(1)}, bf16[96,2048]{1,0:T(8,128)(2,1)}, u32[]{:S(2)}) copy-start(bf16[96,2048]{1,0:T(8,128)(2,1)} %param.19) | copy-start | bytes 1179652
  0.6 6.8 %copy-start.1 = (f32[2048]{0:T(1024)S(1)}, f32[2048]{0:T(1024)}, u32[]{:S(2)}) copy-start(f32[2048]{0:T(1024)} %param.20) | copy-start | bytes 24580

commit v2 on v1

v2 whole, which is shorter than its diff:
```python
import functools

import jax
import jax.numpy as jnp
from jax import lax
from jax.experimental import pallas as pl
from jax.experimental.pallas import tpu as pltpu
from jax.sharding import Mesh
from jax.sharding import PartitionSpec as P

EP = ("ep_0", "ep_1", "ep_2")
EP_TP = ("ep_0", "ep_1", "ep_2", "tp")
MESH = pl.DeviceIdType.MESH

NZ, NY, NC, NX = 8, 4, 2, 4
CHUNKS = NY
BLOCKS = NZ * NC
CAP = 4
QUARTERS = 4
GROUP = BLOCKS * CAP
NEG_LARGE = -1e30
F32 = jnp.float32
BF16 = jnp.bfloat16


def dz_order():
    return (1, 7, 2, 6, 3, 5, 4, 0)


def kernel(
    tok_ref,
    ng_ref,
    routes_ref,
    rw_ref,
    q_in,
    k_ref,
    v_ref,
    mix_ref,
    gain_ref,
    ow_hbm,
    gw_hbm,
    uw_hbm,
    dw_hbm,
    attn_o,
    moe_o,
    gw,
    uw,
    dw,
    ow_ref,
    outbound,
    q_ref,
    comb_ref,
    kbuf,
    vbuf,
    perm,
    perm_t,
    arr,
    xb,
    hid,
    part,
    opp,
    fin,
    back,
    ret,
    rows_ref,
    m_ref,
    acc_ref,
    att_ref,
    ap,
    ar,
    w_sem,
    kv_own,
    z_send,
    z_recv,
    y_send,
    y_recv,
    h_send,
    h_recv,
    c_send,
    c_recv,
    a_send,
    a_recv,
    x_send,
    x_recv,
    f_send,
    f_recv,
    s1_send,
    s1_recv,
    s2_send,
    fin_recv,
    b_send,
    r_recv,
    at_send,
    at_recv,
):
    z = lax.axis_index("ep_0")
    y = lax.axis_index("ep_1")
    c = lax.axis_index("ep_2")
    x = lax.axis_index("tp")
    me = z * (NY * NC) + y * NC + c
    right = {"tp": lax.rem(x + 1, NX)}
    left = {"tp": lax.rem(x + NX - 1, NX)}
    y_up = {"ep_1": lax.rem(y + 1, NY)}
    y_down = {"ep_1": lax.rem(y + NY - 1, NY)}
    ym1 = lax.rem(y + NY - 1, NY)
    yp1 = lax.rem(y + 1, NY)
    partner = {"ep_2": 1 - c}

    def rcopy(src, dst, ssem, rsem, dev):
        return pltpu.make_async_remote_copy(
            src_ref=src, dst_ref=dst, send_sem=ssem, recv_sem=rsem, device_id=dev, device_id_type=MESH
        )

    barrier = pltpu.get_barrier_semaphore()

    def greet(g, carry):
        for dz in range(NZ):
            for dc in range(NC):

                def go():
                    pl.semaphore_signal(
                        barrier,
                        inc=1,
                        device_id={
                            "ep_0": lax.rem(z + dz, NZ),
                            "ep_1": lax.rem(y + g, NY),
                            "ep_2": (1 - c) if dc else c,
                        },
                        device_id_type=MESH,
                    )

                if dz == 0 and dc == 0:
                    pl.when(g > 0)(go)
                else:
                    go()
        return carry

    lax.fori_loop(0, CHUNKS, greet, 0)
    for r in range(1, NX):
        pl.semaphore_signal(barrier, inc=1, device_id={"tp": lax.rem(x + r, NX)}, device_id_type=MESH)

    kv = ((k_ref, kbuf, 0), (v_ref, vbuf, 1))
    for ref, buf, j in kv:
        pltpu.make_async_copy(ref, buf.at[z, y, c], kv_own.at[j]).start()
    weights = [
        pltpu.make_async_copy(s, d, w_sem.at[i])
        for i, (s, d) in enumerate(((gw_hbm, gw), (uw_hbm, uw), (dw_hbm, dw), (ow_hbm, ow_ref)))
    ]
    for copy in weights:
        copy.start()

    size = BLOCKS * QUARTERS * CAP
    r_io = lax.broadcasted_iota(jnp.int32, (size, size), 0)
    c_io = lax.broadcasted_iota(jnp.int32, (size, size), 1)

    def packed_place(r):
        return (r % GROUP) // CAP * (QUARTERS * CAP) + r // GROUP * CAP + r % CAP

    perm[...] = (packed_place(r_io) == c_io).astype(BF16)
    perm_t[...] = (packed_place(c_io) == r_io).astype(BF16)

    tok = tok_ref.shape[0]
    slots = CHUNKS * GROUP
    sub = lax.broadcasted_iota(jnp.int32, (tok, tok), 0)
    lane = lax.broadcasted_iota(jnp.int32, (tok, tok), 1)
    same = sub == lane

    def as_row(col, zero):
        return jnp.sum(jnp.where(same, jnp.broadcast_to(col, (tok, tok)), zero), axis=0, keepdims=True)

    def as_col(row, zero):
        return jnp.sum(jnp.where(same, jnp.broadcast_to(row, (tok, tok)), zero), axis=1, keepdims=True)

    cols = [routes_ref[:, k : k + 1] for k in range(2)]
    slot_iota = lax.broadcasted_iota(jnp.int32, (slots, tok), 0)
    place_iota = lax.broadcasted_iota(jnp.int32, (tok, slots), 1)
    dispatch = jnp.zeros((slots, tok), F32)
    comb = jnp.zeros((tok, slots), F32)
    for k in range(2):
        e = as_row(cols[k], 0)
        rank = jnp.sum(
            jnp.where(sub < lane, (cols[0] == e).astype(jnp.int32) + (cols[1] == e).astype(jnp.int32), 0),
            axis=0,
            keepdims=True,
        )
        ez, ey, ec = e >> 3, (e >> 1) & (NY - 1), e & (NC - 1)
        offset = ((ey + NY - y) & (NY - 1)) * BLOCKS + ((ez + NZ - z) & (NZ - 1)) * NC + ((ec + c) & (NC - 1))
        slot = offset * CAP + rank
        dispatch = dispatch + (slot_iota == slot).astype(F32)
        comb = comb + jnp.where(place_iota == as_col(slot, 0), rw_ref[:, k : k + 1], 0.0)
    high = comb.astype(BF16)
    comb_ref[:tok] = high
    comb_ref[tok:] = (comb - high.astype(F32)).astype(BF16)
    widened = tok_ref[...].astype(F32)
    normed = (
        widened * lax.rsqrt(jnp.mean(widened * widened, axis=1, keepdims=True) + 1e-06) * ng_ref[...]
    ).astype(BF16)
    ordered = jnp.dot(dispatch.astype(BF16), normed, preferred_element_type=F32).astype(BF16)
    width = ordered.shape[1] // QUARTERS

    def pack(block):
        tall = jnp.concatenate([block[:, kq * width : (kq + 1) * width] for kq in range(QUARTERS)], axis=0)
        turned = jnp.dot(perm_t[...], tall, preferred_element_type=F32).astype(BF16)
        return turned.reshape(BLOCKS, QUARTERS * CAP, width)

    for g in range(CHUNKS):
        outbound[g] = pack(ordered[g * GROUP : (g + 1) * GROUP])
    heads = q_in.shape[1] // 128
    map_lane = lax.broadcasted_iota(jnp.int32, (q_in.shape[0], 128), 1) < 64
    for h in range(heads):
        scaled = (q_in[:, h * 128 : (h + 1) * 128].astype(F32) * 0.125)
        q_ref[h] = jnp.where(map_lane, scaled, 0.0).astype(BF16)
        q_ref[heads + h] = jnp.where(map_lane, 0.0, scaled).astype(BF16)

    for ref, buf, j in kv:
        pltpu.make_async_copy(ref, buf.at[z, y, c], kv_own.at[j]).wait()
    with jax.named_scope("barrier"):
        pl.semaphore_wait(barrier, CHUNKS * BLOCKS - 1 + NX - 1)

    z_up = {"ep_0": lax.rem(z + 1, NZ)}
    z_down = {"ep_0": lax.rem(z + NZ - 1, NZ)}

    def zb(k):
        return lax.rem(z + NZ + k, NZ)

    def z_copies(k):
        ups = [rcopy(b.at[zb(1 - k), y, c], b.at[zb(1 - k), y, c], z_send.at[k - 1, 0, j], z_recv.at[k - 1, 0, j], z_up)
               for _, b, j in kv if k < 4 or j == 0]
        downs = [rcopy(b.at[zb(k - 1), y, c], b.at[zb(k - 1), y, c], z_send.at[k - 1, 1, j], z_recv.at[k - 1, 1, j], z_down)
                 for _, b, j in kv if k < 4 or j == 1]
        return ups + downs

    def z_blocks(k):
        return (0,) if k == 0 else (4,) if k == 4 else (-k, k)

    def y_copies(k):
        out = []
        for n, dz in enumerate(z_blocks(k)):
            for _, b, j in kv:
                ref = b.at[zb(dz), y, c]
                for d, dev in enumerate((y_up, y_down)):
                    out.append(rcopy(ref, ref, y_send.at[k, n, d, j], y_recv.at[k, n, d, j], dev))
        return out

    def hop_copies(k):
        out = []
        for n, dz in enumerate(z_blocks(k)):
            lo = kbuf.at[zb(dz), ym1, c]
            out.append(rcopy(lo, lo, h_send.at[k, n, 0], h_recv.at[k, n, 0], y_up))
            hi = vbuf.at[zb(dz), yp1, c]
            out.append(rcopy(hi, hi, h_send.at[k, n, 1], h_recv.at[k, n, 1], y_down))
        return out

    def core_copies():
        return [rcopy(b.at[:, :, c], b.at[:, :, c], c_send.at[j], c_recv.at[j], partner) for _, b, j in kv]

    def start(copies):
        for copy in copies:
            copy.start()

    def landed(copies):
        for copy in copies:
            copy.wait_recv()

    def send_rows(g):
        for dz in dz_order():
            for dc in range(NC):
                i = dz * NC + dc
                if isinstance(g, int) and g == 0 and i == 0:
                    pltpu.make_async_copy(outbound.at[0, 0], arr.at[0, 0], a_recv.at[0]).start()
                    continue
                dev = {
                    "ep_0": lax.rem(z + dz, NZ),
                    "ep_1": lax.rem(y + g, NY),
                    "ep_2": (1 - c) if dc else c,
                }
                rcopy(outbound.at[g, i], arr.at[g, i], a_send.at[0], a_recv.at[g], dev).start()

    start(z_copies(1))
    start(y_copies(0))
    send_rows(0)
    send_rows(1)
    with jax.named_scope("kv_1"):
        landed(z_copies(1))
    start(z_copies(2))
    start(y_copies(1))
    send_rows(2)

    def relayout_in(src, g, store):
        tile = src[g].reshape(size, width)
        turned = jnp.dot(perm[...], tile, preferred_element_type=F32).astype(BF16)
        for kq in range(QUARTERS):
            store(kq, turned[kq * GROUP : (kq + 1) * GROUP])

    def gather_first(g):
        pltpu.make_async_copy(arr.at[g], arr.at[g], a_recv.at[g]).wait()

        def store(kq, value):
            xb[g, 0, :, kq * width : (kq + 1) * width] = value

        relayout_in(arr, g, store)
        rcopy(xb.at[g, 0], xb.at[g, 1], x_send.at[0, g], x_recv.at[0, g], right).start()
        rcopy(xb.at[g, 0], xb.at[g, 2], x_send.at[1, g], x_recv.at[1, g], left).start()

    top, low = pl.ds(0, GROUP // 2), pl.ds(GROUP // 2, GROUP // 2)

    def gather_second(g):
        rcopy(xb.at[g, 0], xb.at[g, 1], x_send.at[0, g], x_recv.at[0, g], right).wait_recv()
        rcopy(xb.at[g, 1, top], xb.at[g, 3, top], f_send.at[0, g], f_recv.at[0, g], right).start()
        rcopy(xb.at[g, 0], xb.at[g, 2], x_send.at[1, g], x_recv.at[1, g], left).wait_recv()
        rcopy(xb.at[g, 2, low], xb.at[g, 3, low], f_send.at[1, g], f_recv.at[1, g], left).start()

    ffe = gw.shape[1]
    model = gw.shape[0]
    rows = NX * GROUP

    def experts(g):
        rcopy(xb.at[g, 1, top], xb.at[g, 3, top], f_send.at[0, g], f_recv.at[0, g], right).wait_recv()
        rcopy(xb.at[g, 2, low], xb.at[g, 3, low], f_send.at[1, g], f_recv.at[1, g], left).wait_recv()

        @pl.when(g == 0)
        def _():
            for copy in weights[:3]:
                copy.wait()

        inputs = xb[g].reshape(rows, model)
        for n in range(0, ffe, 256):
            w = min(256, ffe - n)
            gate = jnp.dot(inputs, gw[:, n : n + w], preferred_element_type=F32)
            up = jnp.dot(inputs, uw[:, n : n + w], preferred_element_type=F32)
            hid[:, n : n + w] = (gate / (1.0 + jnp.exp(-gate)) * up).astype(BF16)
        hidden = hid[...]
        for n in range(0, model, 256):
            part[g, :, :, n : n + 256] = (
                jnp.dot(hidden, dw[:, n : n + 256], preferred_element_type=F32).astype(BF16).reshape(NX, GROUP, 256)
            )
        rcopy(part.at[g, 3, top], opp.at[g, 0], s1_send.at[0, g], s1_recv.at[0, g], right).start()
        rcopy(part.at[g, 3, low], opp.at[g, 1], s1_send.at[1, g], s1_recv.at[1, g], left).start()
        rcopy(part.at[g, 2, low], fin.at[g, 0, low], s2_send.at[0, g], fin_recv.at[0, g], right).start()
        rcopy(part.at[g, 1, top], fin.at[g, 1, top], s2_send.at[1, g], fin_recv.at[1, g], left).start()

    def sum_second(g):
        rcopy(part.at[g, 3, top], opp.at[g, 0], s1_send.at[0, g], s1_recv.at[0, g], right).wait_recv()
        part[g, 2, : GROUP // 2] = (part[g, 2, : GROUP // 2].astype(F32) + opp[g, 0].astype(F32)).astype(BF16)
        rcopy(part.at[g, 2, top], fin.at[g, 0, top], s2_send.at[2, g], fin_recv.at[2, g], right).start()
        rcopy(part.at[g, 3, low], opp.at[g, 1], s1_send.at[1, g], s1_recv.at[1, g], left).wait_recv()
        part[g, 1, GROUP // 2 :] = (part[g, 1, GROUP // 2 :].astype(F32) + opp[g, 1].astype(F32)).astype(BF16)
        rcopy(part.at[g, 1, low], fin.at[g, 1, low], s2_send.at[3, g], fin_recv.at[3, g], left).start()

    def sum_last(g):
        rcopy(part.at[g, 2, low], fin.at[g, 0, low], s2_send.at[0, g], fin_recv.at[0, g], right).wait_recv()
        rcopy(part.at[g, 1, top], fin.at[g, 1, top], s2_send.at[1, g], fin_recv.at[1, g], left).wait_recv()
        rcopy(part.at[g, 2, top], fin.at[g, 0, top], s2_send.at[2, g], fin_recv.at[2, g], right).wait_recv()
        rcopy(part.at[g, 1, low], fin.at[g, 1, low], s2_send.at[3, g], fin_recv.at[3, g], left).wait_recv()
        total = (part[g, 0].astype(F32) + fin[g, 0].astype(F32) + fin[g, 1].astype(F32)).astype(BF16)
        back[g] = pack(total)
        for dz in dz_order():
            for dc in range(NC):
                i = dz * NC + dc

                def go():
                    dev = {
                        "ep_0": lax.rem(z + NZ - dz, NZ),
                        "ep_1": lax.rem(y + NY - g, NY),
                        "ep_2": (1 - c) if dc else c,
                    }
                    rcopy(back.at[g, i], ret.at[g, i], b_send.at[0], r_recv.at[g], dev).start()

                if i == 0:
                    pl.when(g > 0)(go)

                    @pl.when(g == 0)
                    def _():
                        pltpu.make_async_copy(back.at[0, 0], ret.at[0, 0], r_recv.at[0]).start()

                else:
                    go()

    ta = q_ref.shape[1]
    span = NY * NC * ta

    def attend_plane(t, masked):
        kc = kbuf[t].reshape(span, kbuf.shape[-1])
        vc = jnp.concatenate([vbuf[t].reshape(span, vbuf.shape[-1]), jnp.ones((span, 128), BF16)], axis=1)
        for r in range(2 * heads):
            s = lax.dot_general(q_ref[r], kc, (((1,), (1,)), ((), ())), preferred_element_type=F32)
            if masked:
                kpos = t * span + lax.broadcasted_iota(jnp.int32, s.shape, 1)
                qpos = me * ta + lax.broadcasted_iota(jnp.int32, s.shape, 0)
                s = jnp.where(kpos <= qpos, s, NEG_LARGE)
            old = m_ref[r][:, :1]
            new = jnp.maximum(old, jnp.max(s, axis=1, keepdims=True))
            p = jnp.exp(s - new)
            scale = jnp.exp(old - new)
            m_ref[r] = jnp.broadcast_to(new, m_ref.shape[1:])
            acc_ref[r] = acc_ref[r] * scale + jnp.dot(p.astype(BF16), vc, preferred_element_type=F32)

    def attend_some(first, end):
        def step(t, carry):
            attend_plane(t, False)
            return carry

        lax.fori_loop(first, jnp.maximum(first, jnp.minimum(end, z)), step, 0)

    def attend_first():
        with jax.named_scope("wait_kv"):
            landed(core_copies())
        m_ref[...] = jnp.full(m_ref.shape, NEG_LARGE, F32)
        acc_ref[...] = jnp.zeros(acc_ref.shape, F32)
        attend_some(0, 3)

    def attend_last():
        attend_plane(z, True)
        for h in range(heads):
            one, two = acc_ref[h], acc_ref[heads + h]
            blended = one[:, :128] / one[:, 128:] - mix_ref[h] * (two[:, :128] / two[:, 128:])
            normed = (
                blended * lax.rsqrt(jnp.mean(blended * blended, axis=1, keepdims=True) + 1e-05) * gain_ref[...]
            ).astype(BF16)
            att_ref[:, :, h * 128 : (h + 1) * 128] = normed.reshape(NX, ta // NX, 128)
        weights[3].wait()
        for r in range(NX):
            j = lax.rem(x + r, NX)
            ap[r] = jnp.dot(att_ref[j], ow_ref[...], preferred_element_type=F32).astype(BF16)
            if r:
                rcopy(ap.at[r], ar.at[r - 1], at_send.at[r - 1], at_recv.at[r - 1], {"tp": j}).start()

    def main(s, carry):
        @pl.when((s >= 4) & (s < CHUNKS + 4))
        def _():
            with jax.named_scope("sum_last"):
                sum_last(s - 4)

        @pl.when((s >= 3) & (s < CHUNKS + 3))
        def _():
            with jax.named_scope("sum_second"):
                sum_second(s - 3)

        @pl.when(s < CHUNKS)
        def _():
            with jax.named_scope("gather_first"):
                gather_first(s)

        @pl.when((s >= 1) & (s < CHUNKS + 1))
        def _():
            with jax.named_scope("gather_second"):
                gather_second(s - 1)

        @pl.when(s == 0)
        def _():
            with jax.named_scope("kv_2"):
                landed(z_copies(2))
                start(z_copies(3))
                start(y_copies(2))
                send_rows(3)
                landed(y_copies(0))
                start(hop_copies(0))

        @pl.when(s == 1)
        def _():
            with jax.named_scope("kv_3"):
                landed(z_copies(3))
                start(z_copies(4))
                start(y_copies(3))
                landed(y_copies(1))
                start(hop_copies(1))

        @pl.when(s == 2)
        def _():
            with jax.named_scope("kv_4"):
                landed(z_copies(4))
                start(y_copies(4))
                landed(y_copies(2))
                start(hop_copies(2))

        @pl.when(s == 3)
        def _():
            with jax.named_scope("kv_5"):
                for k in (3, 4):
                    landed(y_copies(k))
                    start(hop_copies(k))

        @pl.when(s == 4)
        def _():
            with jax.named_scope("kv_6"):
                for k in range(5):
                    landed(hop_copies(k))
                start(core_copies())

        @pl.when((s >= 2) & (s < CHUNKS + 2))
        def _():
            with jax.named_scope("experts"):
                experts(s - 2)

        @pl.when(s == CHUNKS)
        def _():
            with jax.named_scope("attend_1"):
                attend_first()

        @pl.when(s == CHUNKS + 1)
        def _():
            with jax.named_scope("attend_2"):
                attend_some(3, 5)

        @pl.when(s == CHUNKS + 2)
        def _():
            with jax.named_scope("attend_3"):
                attend_some(5, NZ)
                attend_last()

        return carry

    lax.fori_loop(0, CHUNKS + 4, main, 0)

    for r in range(1, NX):
        rcopy(ap.at[r], ar.at[r - 1], at_send.at[r - 1], at_recv.at[r - 1], right).wait_recv()
    total = ap[0].astype(F32)
    for r in range(1, NX):
        total = total + ar[r - 1].astype(F32)
    attn_o[...] = total.astype(BF16)

    def collect(g, carry):
        with jax.named_scope("wait_ret"):
            pltpu.make_async_copy(ret.at[g], ret.at[g], r_recv.at[g]).wait()

        def store(kq, value):
            rows_ref[pl.ds(pl.multiple_of(g * GROUP, GROUP), GROUP), kq * width : (kq + 1) * width] = value

        relayout_in(ret, g, store)
        return carry

    lax.fori_loop(0, CHUNKS, collect, 0)
    tokens = tok
    for kq in range(QUARTERS):
        both = jnp.dot(comb_ref[...], rows_ref[:, kq * width : (kq + 1) * width], preferred_element_type=F32)
        moe_o[:, kq * width : (kq + 1) * width] = (both[:tokens] + both[tokens:]).astype(BF16)

    for g in range(CHUNKS):
        for copy in (
            rcopy(xb.at[g, 0], xb.at[g, 1], x_send.at[0, g], x_recv.at[0, g], right),
            rcopy(xb.at[g, 0], xb.at[g, 2], x_send.at[1, g], x_recv.at[1, g], left),
            rcopy(xb.at[g, 1, top], xb.at[g, 3, top], f_send.at[0, g], f_recv.at[0, g], right),
            rcopy(xb.at[g, 2, low], xb.at[g, 3, low], f_send.at[1, g], f_recv.at[1, g], left),
            rcopy(part.at[g, 3, top], opp.at[g, 0], s1_send.at[0, g], s1_recv.at[0, g], right),
            rcopy(part.at[g, 3, low], opp.at[g, 1], s1_send.at[1, g], s1_recv.at[1, g], left),
            rcopy(part.at[g, 2, low], fin.at[g, 0, low], s2_send.at[0, g], fin_recv.at[0, g], right),
            rcopy(part.at[g, 1, top], fin.at[g, 1, top], s2_send.at[1, g], fin_recv.at[1, g], left),
            rcopy(part.at[g, 2, top], fin.at[g, 0, top], s2_send.at[2, g], fin_recv.at[2, g], right),
            rcopy(part.at[g, 1, low], fin.at[g, 1, low], s2_send.at[3, g], fin_recv.at[3, g], left),
        ):
            copy.wait_send()
    for r in range(1, NX):
        rcopy(ap.at[r], ar.at[r - 1], at_send.at[r - 1], at_recv.at[r - 1], right).wait_send()
    for k in range(1, 5):
        for copy in z_copies(k):
            copy.wait_send()
    for k in range(5):
        for copy in y_copies(k) + hop_copies(k):
            copy.wait_send()
    for copy in core_copies():
        copy.wait_send()
    for sem, buf in ((a_send, outbound), (b_send, back)):
        for g in range(CHUNKS):
            blocks = buf.at[g, pl.ds(1, BLOCKS - 1)] if g == 0 else buf.at[g]
            rcopy(blocks, blocks, sem.at[0], r_recv.at[g], right).wait_send()


def body(
    queries,
    keys,
    values,
    mix_scale,
    head_gain,
    out_weight,
    moe_input,
    norm_gain,
    routes,
    route_weights,
    gate_weight,
    up_weight,
    down_weight,
):
    ta, heads, qd = queries.shape
    tok, model = moe_input.shape
    ffe = gate_weight.shape[2]
    vd = values.shape[2]
    width = model // QUARTERS
    slots = CHUNKS * GROUP
    vmem = pl.BlockSpec(memory_space=pltpu.VMEM)
    hbm = pl.BlockSpec(memory_space=pl.ANY)
    dma = pltpu.SemaphoreType.DMA
    size = BLOCKS * QUARTERS * CAP
    attn_out, moe_out = pl.pallas_call(
        kernel,
        out_shape=(
            jax.ShapeDtypeStruct((ta // NX, model), BF16),
            jax.ShapeDtypeStruct((tok, model), BF16),
        ),
        in_specs=[vmem] * 5 + [vmem] * 2 + [pl.BlockSpec(memory_space=pltpu.SMEM), vmem] + [hbm] * 4,
        out_specs=(vmem, vmem),
        scratch_shapes=[
            pltpu.VMEM((model, ffe), BF16),
            pltpu.VMEM((model, ffe), BF16),
            pltpu.VMEM((ffe, model), BF16),
            pltpu.VMEM((heads * vd, model), BF16),
            pltpu.VMEM((CHUNKS, BLOCKS, QUARTERS * CAP, width), BF16),
            pltpu.VMEM((2 * heads, ta, qd), BF16),
            pltpu.VMEM((2 * tok, slots), BF16),
            pltpu.VMEM((NZ, NY, NC, ta, qd), BF16),
            pltpu.VMEM((NZ, NY, NC, ta, vd), BF16),
            pltpu.VMEM((size, size), BF16),
            pltpu.VMEM((size, size), BF16),
            pltpu.VMEM((CHUNKS, BLOCKS, QUARTERS * CAP, width), BF16),
            pltpu.VMEM((CHUNKS, NX, GROUP, model), BF16),
            pltpu.VMEM((NX * GROUP, ffe), BF16),
            pltpu.VMEM((CHUNKS, NX, GROUP, model), BF16),
            pltpu.VMEM((CHUNKS, 2, GROUP // 2, model), BF16),
            pltpu.VMEM((CHUNKS, 2, GROUP, model), BF16),
            pltpu.VMEM((CHUNKS, BLOCKS, QUARTERS * CAP, width), BF16),
            pltpu.VMEM((CHUNKS, BLOCKS, QUARTERS * CAP, width), BF16),
            pltpu.VMEM((slots, model), BF16),
            pltpu.VMEM((2 * heads, ta, 128), F32),
            pltpu.VMEM((2 * heads, ta, 2 * vd), F32),
            pltpu.VMEM((NX, ta // NX, heads * vd), BF16),
            pltpu.VMEM((NX, ta // NX, model), BF16),
            pltpu.VMEM((NX - 1, ta // NX, model), BF16),
            dma((4,)),
            dma((2,)),
            dma((4, 2, 2)),
            dma((4, 2, 2)),
            dma((5, 2, 2, 2)),
            dma((5, 2, 2, 2)),
            dma((5, 2, 2)),
            dma((5, 2, 2)),
            dma((2,)),
            dma((2,)),
            dma((1,)),
            dma((CHUNKS,)),
            dma((2, CHUNKS)),
            dma((2, CHUNKS)),
            dma((2, CHUNKS)),
            dma((2, CHUNKS)),
            dma((2, CHUNKS)),
            dma((2, CHUNKS)),
            dma((4, CHUNKS)),
            dma((4, CHUNKS)),
            dma((1,)),
            dma((CHUNKS,)),
            dma((NX - 1,)),
            dma((NX - 1,)),
        ],
        compiler_params=pltpu.CompilerParams(collective_id=0, has_side_effects=True, vmem_limit_bytes=62 * 1024 * 1024),
    )(
        moe_input,
        norm_gain.reshape(1, model),
        routes,
        route_weights,
        queries.reshape(ta, heads * qd),
        keys.reshape(ta, qd),
        values.reshape(ta, vd),
        mix_scale,
        head_gain.reshape(1, vd),
        out_weight.reshape(heads * vd, model),
        gate_weight[0],
        up_weight[0],
        down_weight[0],
    )
    return (attn_out, moe_out)


def solution(mesh):
    split = Mesh(mesh.devices.reshape(NZ, NY, NC, NX), EP_TP)
    placed = (
        P(EP, "tp", None),
        P(EP, "tp", None),
        P(EP, "tp", None),
        P("tp"),
        P(),
        P("tp", None, None),
        P(EP_TP, None),
        P(),
        P(EP_TP, None),
        P(EP_TP, None),
        P(EP, None, "tp"),
        P(EP, None, "tp"),
        P(EP, "tp", None),
    )
    return jax.shard_map(
        body,
        mesh=split,
        in_specs=placed,
        out_specs=(P(EP_TP, None), P(EP_TP, None)),
        check_vma=False,
    )
```

time: 177 us -> 120 us (0.68)
  Pallas kernels: 163 us -> 112 us
  other arithmetic: 5.55 us -> 0 us
  local copies, waits for them, and re-layouts: 5.11 us -> 7.72 us
  matrix products: 1.99 us -> 0 us
    pallas_call x1, Pallas kernels: 163 us -> 112 us  [body(): pl.pallas_call(kernel, out_shape=(jax.ShapeDtypeStruct((ta // NX, model),...]
    unnamed x7 -> x5, local copies, waits for them, and re-layouts: 4.17 us -> 7.72 us
    reduce_sum x3 -> x0, other arithmetic: 2.21 us -> none  [the longest x1 1.22 us: body(): jnp.mean(widened * widened, axis=-1, keepdims=True) + 1e-06]
    dot_general x1 -> x0, matrix products: 1.99 us -> none  [body(): jnp.dot(dispatch, stacked, preferred_element_type=F32).astype(BF16)]
where the time goes in v2:
time: 120 us
  Pallas kernels  112 us (93%)
  local copies, waits for them, and re-layouts  7.72 us (6%)
    pallas_call x1, Pallas kernels, body(): pl.pallas_call(kernel, out_shape=(jax.ShapeDtypeStruct((ta // NX, model),...  112 us
    unnamed x5, local copies, waits for them, and re-layouts  7.72 us

profile of v2, /device:TPU:1, one launch (start us, length us, event | category | flops | bytes accessed | tf_op | source)
XLA Modules:
  0.0 120.1 jit_solution(7901270130765907794)
XLA Ops:
  0.6 1.4 %copy.15.routes_ref = s32[96,2]{1,0:T(8,128)} copy(s32[96,2]{0,1:T(2,128)} %param.21) | data formatting | bytes 1536 | tf_op args[8]
  2.0 1.4 %copy.16.rw_ref = f32[96,2]{1,0:T(8,128)} copy(f32[96,2]{0,1:T(2,128)} %param.22) | data formatting | bytes 1536 | tf_op args[9]
  3.4 1.5 %copy.19 = bf16[24,8,2,128]{3,1,2,0:T(8,128)(2,1)} copy(bf16[24,8,2,128]{3,2,1,0:T(2,128)(2,1)} %bitcast.17) | data formatting | bytes 196608
  5.0 111.7 %shard_map.140 = (bf16[48,2048]{1,0:T(8,128)(2,1)}, bf16[96,2048]{1,0:T(8,128)(2,1)}) custom-call(bf16[96,2048]{1,0:T(8,128)(2,1)} %tok_ref.1, f32[1,2048]{1,0:T(1,128)} %bitcast.20, s32[96,2]{1,0:T(8,128)} %copy.15.routes_ref, f32[96,2]{1,0:T(8,128)} %copy.16.rw_ref, bf16[192,256]{1,0:T(8,128)(2,1)} %bitcast.16, bf16[192,128]{1,0:T(8,128)(2,1)} %bitcast.18, ...), custom_call_target="tpu_custom_call" | custom-call | tf_op jit(solution)/shard_map/pallas_call | solution.py:593
  116.7 1.6 %copy.22 = bf16[48,2048]{1,0:T(8,128)(2,1)} copy(bf16[48,2048]{1,0:T(8,128)(2,1)} %get-tuple-element.4) | data formatting | bytes 393216
  118.3 1.8 %copy.23 = bf16[96,2048]{1,0:T(8,128)(2,1)} copy(bf16[96,2048]{1,0:T(8,128)(2,1)} %get-tuple-element.5) | data formatting | bytes 786432

commit v3 on v2

--- a/solution.py
+++ b/solution.py
@@ -13,8 +13,8 @@
 MESH = pl.DeviceIdType.MESH
 
 NZ, NY, NC, NX = 8, 4, 2, 4
-CHUNKS = NY
-BLOCKS = NZ * NC
+CHUNKS = 4
+BLOCKS = NZ * NY * NC // CHUNKS
 CAP = 4
 QUARTERS = 4
 GROUP = BLOCKS * CAP
@@ -23,8 +23,21 @@
 BF16 = jnp.bfloat16
 
 
-def dz_order():
-    return (1, 7, 2, 6, 3, 5, 4, 0)
+def offsets():
+    out = [(0, dy, dc) for dy in range(NY) for dc in range(NC)]
+    for k in (1, 2, 3):
+        out += [(dz, dy, dc) for dc in range(NC) for dy in range(NY) for dz in (k, NZ - k)]
+    return out + [(NZ // 2, dy, dc) for dy in range(NY) for dc in range(NC)]
+
+
+OFFSETS = offsets()
+
+
+def place_of(dz, dy, dc):
+    k = jnp.minimum(dz, NZ - dz)
+    ends = dy * NC + dc
+    between = 16 * k - 8 + dc * 8 + dy * 2 + (dz > NZ // 2).astype(jnp.int32)
+    return jnp.where(k == 0, ends, jnp.where(k == NZ // 2, 56 + ends, between))
 
 
 def kernel(
@@ -67,6 +80,7 @@
     acc_ref,
     att_ref,
     ap,
+    ao,
     ar,
     w_sem,
     kv_own,
@@ -113,29 +127,16 @@
 
     barrier = pltpu.get_barrier_semaphore()
 
-    def greet(g, carry):
-        for dz in range(NZ):
-            for dc in range(NC):
-
-                def go():
-                    pl.semaphore_signal(
-                        barrier,
-                        inc=1,
-                        device_id={
-                            "ep_0": lax.rem(z + dz, NZ),
-                            "ep_1": lax.rem(y + g, NY),
-                            "ep_2": (1 - c) if dc else c,
-                        },
-                        device_id_type=MESH,
-                    )
-
-                if dz == 0 and dc == 0:
-                    pl.when(g > 0)(go)
-                else:
-                    go()
-        return carry
-
-    lax.fori_loop(0, CHUNKS, greet, 0)
+    def at_offset(i):
+        dz, dy, dc = OFFSETS[i]
+        return {"ep_0": lax.rem(z + dz, NZ), "ep_1": lax.rem(y + dy, NY), "ep_2": (1 - c) if dc else c}
+
+    def from_offset(i):
+        dz, dy, dc = OFFSETS[i]
+        return {"ep_0": lax.rem(z + NZ - dz, NZ), "ep_1": lax.rem(y + NY - dy, NY), "ep_2": (1 - c) if dc else c}
+
+    for i in range(CHUNKS * BLOCKS - 1, 0, -1):
+        pl.semaphore_signal(barrier, inc=1, device_id=at_offset(i), device_id_type=MESH)
     for r in range(1, NX):
         pl.semaphore_signal(barrier, inc=1, device_id={"tp": lax.rem(x + r, NX)}, device_id_type=MESH)
 
@@ -165,29 +166,27 @@
     lane = lax.broadcasted_iota(jnp.int32, (tok, tok), 1)
     same = sub == lane
 
-    def as_row(col, zero):
-        return jnp.sum(jnp.where(same, jnp.broadcast_to(col, (tok, tok)), zero), axis=0, keepdims=True)
-
     def as_col(row, zero):
         return jnp.sum(jnp.where(same, jnp.broadcast_to(row, (tok, tok)), zero), axis=1, keepdims=True)
 
-    cols = [routes_ref[:, k : k + 1] for k in range(2)]
+    named = [routes_ref[k : k + 1, :] for k in range(2)]
+    cols = [as_col(row, 0) for row in named]
     slot_iota = lax.broadcasted_iota(jnp.int32, (slots, tok), 0)
     place_iota = lax.broadcasted_iota(jnp.int32, (tok, slots), 1)
     dispatch = jnp.zeros((slots, tok), F32)
     comb = jnp.zeros((tok, slots), F32)
     for k in range(2):
-        e = as_row(cols[k], 0)
+        e = named[k]
         rank = jnp.sum(
             jnp.where(sub < lane, (cols[0] == e).astype(jnp.int32) + (cols[1] == e).astype(jnp.int32), 0),
             axis=0,
             keepdims=True,
         )
         ez, ey, ec = e >> 3, (e >> 1) & (NY - 1), e & (NC - 1)
-        offset = ((ey + NY - y) & (NY - 1)) * BLOCKS + ((ez + NZ - z) & (NZ - 1)) * NC + ((ec + c) & (NC - 1))
+        offset = place_of((ez + NZ - z) & (NZ - 1), (ey + NY - y) & (NY - 1), (ec + c) & (NC - 1))
         slot = offset * CAP + rank
         dispatch = dispatch + (slot_iota == slot).astype(F32)
-        comb = comb + jnp.where(place_iota == as_col(slot, 0), rw_ref[:, k : k + 1], 0.0)
+        comb = comb + jnp.where(place_iota == as_col(slot, 0), as_col(rw_ref[k : k + 1, :], 0.0), 0.0)
     high = comb.astype(BF16)
     comb_ref[:tok] = high
     comb_ref[tok:] = (comb - high.astype(F32)).astype(BF16)
@@ -205,13 +204,6 @@
 
     for g in range(CHUNKS):
         outbound[g] = pack(ordered[g * GROUP : (g + 1) * GROUP])
-    heads = q_in.shape[1] // 128
-    map_lane = lax.broadcasted_iota(jnp.int32, (q_in.shape[0], 128), 1) < 64
-    for h in range(heads):
-        scaled = (q_in[:, h * 128 : (h + 1) * 128].astype(F32) * 0.125)
-        q_ref[h] = jnp.where(map_lane, scaled, 0.0).astype(BF16)
-        q_ref[heads + h] = jnp.where(map_lane, 0.0, scaled).astype(BF16)
-
     for ref, buf, j in kv:
         pltpu.make_async_copy(ref, buf.at[z, y, c], kv_own.at[j]).wait()
     with jax.named_scope("barrier"):
@@ -263,28 +255,11 @@
             copy.wait_recv()
 
     def send_rows(g):
-        for dz in dz_order():
-            for dc in range(NC):
-                i = dz * NC + dc
-                if isinstance(g, int) and g == 0 and i == 0:
-                    pltpu.make_async_copy(outbound.at[0, 0], arr.at[0, 0], a_recv.at[0]).start()
-                    continue
-                dev = {
-                    "ep_0": lax.rem(z + dz, NZ),
-                    "ep_1": lax.rem(y + g, NY),
-                    "ep_2": (1 - c) if dc else c,
-                }
-                rcopy(outbound.at[g, i], arr.at[g, i], a_send.at[0], a_recv.at[g], dev).start()
-
-    start(z_copies(1))
-    start(y_copies(0))
-    send_rows(0)
-    send_rows(1)
-    with jax.named_scope("kv_1"):
-        landed(z_copies(1))
-    start(z_copies(2))
-    start(y_copies(1))
-    send_rows(2)
+        for i in range(BLOCKS):
+            if g == 0 and i == 0:
+                pltpu.make_async_copy(outbound.at[0, 0], arr.at[0, 0], a_recv.at[0]).start()
+            else:
+                rcopy(outbound.at[g, i], arr.at[g, i], a_send.at[0], a_recv.at[g], at_offset(g * BLOCKS + i)).start()
 
     def relayout_in(src, g, store):
         tile = src[g].reshape(size, width)
@@ -334,6 +309,8 @@
             part[g, :, :, n : n + 256] = (
                 jnp.dot(hidden, dw[:, n : n + 256], preferred_element_type=F32).astype(BF16).reshape(NX, GROUP, 256)
             )
+
+    def sum_first(g):
         rcopy(part.at[g, 3, top], opp.at[g, 0], s1_send.at[0, g], s1_recv.at[0, g], right).start()
         rcopy(part.at[g, 3, low], opp.at[g, 1], s1_send.at[1, g], s1_recv.at[1, g], left).start()
         rcopy(part.at[g, 2, low], fin.at[g, 0, low], s2_send.at[0, g], fin_recv.at[0, g], right).start()
@@ -354,27 +331,11 @@
         rcopy(part.at[g, 1, low], fin.at[g, 1, low], s2_send.at[3, g], fin_recv.at[3, g], left).wait_recv()
         total = (part[g, 0].astype(F32) + fin[g, 0].astype(F32) + fin[g, 1].astype(F32)).astype(BF16)
         back[g] = pack(total)
-        for dz in dz_order():
-            for dc in range(NC):
-                i = dz * NC + dc
-
-                def go():
-                    dev = {
-                        "ep_0": lax.rem(z + NZ - dz, NZ),
-                        "ep_1": lax.rem(y + NY - g, NY),
-                        "ep_2": (1 - c) if dc else c,
-                    }
-                    rcopy(back.at[g, i], ret.at[g, i], b_send.at[0], r_recv.at[g], dev).start()
-
-                if i == 0:
-                    pl.when(g > 0)(go)
-
-                    @pl.when(g == 0)
-                    def _():
-                        pltpu.make_async_copy(back.at[0, 0], ret.at[0, 0], r_recv.at[0]).start()
-
-                else:
-                    go()
+        for i in range(BLOCKS):
+            if g == 0 and i == 0:
+                pltpu.make_async_copy(back.at[0, 0], ret.at[0, 0], r_recv.at[0]).start()
+            else:
+                rcopy(back.at[g, i], ret.at[g, i], b_send.at[0], r_recv.at[g], from_offset(g * BLOCKS + i)).start()
 
     ta = q_ref.shape[1]
     span = NY * NC * ta
@@ -402,13 +363,6 @@
 
         lax.fori_loop(first, jnp.maximum(first, jnp.minimum(end, z)), step, 0)
 
-    def attend_first():
-        with jax.named_scope("wait_kv"):
-            landed(core_copies())
-        m_ref[...] = jnp.full(m_ref.shape, NEG_LARGE, F32)
-        acc_ref[...] = jnp.zeros(acc_ref.shape, F32)
-        attend_some(0, 3)
-
     def attend_last():
         attend_plane(z, True)
         for h in range(heads):
@@ -422,118 +376,131 @@
         for r in range(NX):
             j = lax.rem(x + r, NX)
             ap[r] = jnp.dot(att_ref[j], ow_ref[...], preferred_element_type=F32).astype(BF16)
-            if r:
-                rcopy(ap.at[r], ar.at[r - 1], at_send.at[r - 1], at_recv.at[r - 1], {"tp": j}).start()
-
-    def main(s, carry):
-        @pl.when((s >= 4) & (s < CHUNKS + 4))
-        def _():
-            with jax.named_scope("sum_last"):
-                sum_last(s - 4)
-
-        @pl.when((s >= 3) & (s < CHUNKS + 3))
-        def _():
-            with jax.named_scope("sum_second"):
-                sum_second(s - 3)
-
-        @pl.when(s < CHUNKS)
-        def _():
-            with jax.named_scope("gather_first"):
-                gather_first(s)
-
-        @pl.when((s >= 1) & (s < CHUNKS + 1))
-        def _():
-            with jax.named_scope("gather_second"):
-                gather_second(s - 1)
+        start(attend_copies(0))
+
+    side = ow_ref.shape[1] // 2
+    one, two = pl.ds(0, side), pl.ds(side, side)
+
+    def attend_copies(n):
+        if n == 0:
+            return [
+                rcopy(ap.at[2, :, one], ao.at[0], at_send.at[0], at_recv.at[0], right),
+                rcopy(ap.at[2, :, two], ao.at[1], at_send.at[1], at_recv.at[1], left),
+                rcopy(ap.at[1, :, two], ar.at[0, :, two], at_send.at[2], at_recv.at[2], right),
+                rcopy(ap.at[3, :, one], ar.at[1, :, one], at_send.at[3], at_recv.at[3], left),
+            ]
+        return [
+            rcopy(ap.at[1, :, one], ar.at[0, :, one], at_send.at[4], at_recv.at[4], right),
+            rcopy(ap.at[3, :, two], ar.at[1, :, two], at_send.at[5], at_recv.at[5], left),
+        ]
+
+    def attend_second():
+        landed(attend_copies(0)[:2])
+        ap[1, :, :side] = (ap[1, :, :side].astype(F32) + ao[0].astype(F32)).astype(BF16)
+        ap[3, :, side:] = (ap[3, :, side:].astype(F32) + ao[1].astype(F32)).astype(BF16)
+        start(attend_copies(1))
+
+    def run(*steps):
+        for step, *args in steps:
+            with jax.named_scope(step.__name__ + "#" + "_".join(str(v) for v in args)):
+                step(*args)
+
+    def kv_1():
+        landed(z_copies(1))
+        start(z_copies(2))
+        start(y_copies(1))
+
+    def kv_2():
+        landed(z_copies(2))
+        start(z_copies(3))
+        start(y_copies(2))
+        landed(y_copies(0))
+        start(hop_copies(0))
+
+    def kv_3():
+        landed(z_copies(3))
+        start(z_copies(4))
+        start(y_copies(3))
+        landed(y_copies(1))
+        start(hop_copies(1))
+
+    def kv_4():
+        landed(z_copies(4))
+        start(y_copies(4))
+        landed(y_copies(2))
+        start(hop_copies(2))
+
+    def kv_5():
+        for k in (3, 4):
+            landed(y_copies(k))
+            start(hop_copies(k))
+
+    def kv_6():
+        for k in range(5):
+            landed(hop_copies(k))
+        start(core_copies())
+
+    send_rows(0)
+    start(z_copies(1))
+    start(y_copies(0))
+    for g in range(1, CHUNKS):
+        send_rows(g)
+    heads = q_in.shape[1]
+    map_lane = lax.broadcasted_iota(jnp.int32, (q_in.shape[0], 128), 1) < 64
+    with jax.named_scope("q_prep"):
+        for h in range(heads):
+            scaled = q_in[:, h, :].astype(F32) * 0.125
+            q_ref[h] = jnp.where(map_lane, scaled, 0.0).astype(BF16)
+            q_ref[heads + h] = jnp.where(map_lane, 0.0, scaled).astype(BF16)
+    run((gather_first, 0), (gather_first, 1), (kv_1,), (gather_second, 0), (gather_first, 2), (kv_2,), (gather_second, 1))
+
+    def first_half(s, carry):
+        with jax.named_scope("experts"):
+            experts(s)
 
         @pl.when(s == 0)
         def _():
-            with jax.named_scope("kv_2"):
-                landed(z_copies(2))
-                start(z_copies(3))
-                start(y_copies(2))
-                send_rows(3)
-                landed(y_copies(0))
-                start(hop_copies(0))
+            run((gather_first, 3), (kv_3,), (gather_second, 2))
 
         @pl.when(s == 1)
         def _():
-            with jax.named_scope("kv_3"):
-                landed(z_copies(3))
-                start(z_copies(4))
-                start(y_copies(3))
-                landed(y_copies(1))
-                start(hop_copies(1))
+            run((kv_4,), (gather_second, 3))
 
         @pl.when(s == 2)
         def _():
-            with jax.named_scope("kv_4"):
-                landed(z_copies(4))
-                start(y_copies(4))
-                landed(y_copies(2))
-                start(hop_copies(2))
-
-        @pl.when(s == 3)
+            run((sum_first, 2), (kv_5,))
+
+        return carry
+
+    lax.fori_loop(0, CHUNKS, first_half, 0)
+    run((sum_first, 3), (kv_6,), (sum_second, 2), (sum_first, 1))
+    with jax.named_scope("wait_kv"):
+        landed(core_copies())
+    m_ref[...] = jnp.full(m_ref.shape, NEG_LARGE, F32)
+    acc_ref[...] = jnp.zeros(acc_ref.shape, F32)
+
+    def second_half(s, carry):
+        @pl.when(s < z)
         def _():
-            with jax.named_scope("kv_5"):
-                for k in (3, 4):
-                    landed(y_copies(k))
-                    start(hop_copies(k))
+            with jax.named_scope("attend"):
+                attend_plane(s, False)
+
+        @pl.when(s == 1)
+        def _():
+            run((sum_second, 3), (sum_last, 2), (sum_first, 0))
 
         @pl.when(s == 4)
         def _():
-            with jax.named_scope("kv_6"):
-                for k in range(5):
-                    landed(hop_copies(k))
-                start(core_copies())
-
-        @pl.when((s >= 2) & (s < CHUNKS + 2))
-        def _():
-            with jax.named_scope("experts"):
-                experts(s - 2)
-
-        @pl.when(s == CHUNKS)
-        def _():
-            with jax.named_scope("attend_1"):
-                attend_first()
-
-        @pl.when(s == CHUNKS + 1)
-        def _():
-            with jax.named_scope("attend_2"):
-                attend_some(3, 5)
-
-        @pl.when(s == CHUNKS + 2)
-        def _():
-            with jax.named_scope("attend_3"):
-                attend_some(5, NZ)
-                attend_last()
+            run((sum_second, 1), (sum_last, 3))
 
         return carry
 
-    lax.fori_loop(0, CHUNKS + 4, main, 0)
-
-    for r in range(1, NX):
-        rcopy(ap.at[r], ar.at[r - 1], at_send.at[r - 1], at_recv.at[r - 1], right).wait_recv()
-    total = ap[0].astype(F32)
-    for r in range(1, NX):
-        total = total + ar[r - 1].astype(F32)
-    attn_o[...] = total.astype(BF16)
-
-    def collect(g, carry):
-        with jax.named_scope("wait_ret"):
-            pltpu.make_async_copy(ret.at[g], ret.at[g], r_recv.at[g]).wait()
-
-        def store(kq, value):
-            rows_ref[pl.ds(pl.multiple_of(g * GROUP, GROUP), GROUP), kq * width : (kq + 1) * width] = value
-
-        relayout_in(ret, g, store)
-        return carry
-
-    lax.fori_loop(0, CHUNKS, collect, 0)
-    tokens = tok
-    for kq in range(QUARTERS):
-        both = jnp.dot(comb_ref[...], rows_ref[:, kq * width : (kq + 1) * width], preferred_element_type=F32)
-        moe_o[:, kq * width : (kq + 1) * width] = (both[:tokens] + both[tokens:]).astype(BF16)
+    lax.fori_loop(0, NZ - 1, second_half, 0)
+    run((attend_last,), (sum_second, 0), (sum_last, 1), (attend_second,), (sum_last, 0))
+
+    with jax.named_scope("wait_attn"):
+        landed(attend_copies(0)[2:] + attend_copies(1))
+    attn_o[...] = (ap[0].astype(F32) + ar[0].astype(F32) + ar[1].astype(F32)).astype(BF16)
 
     for g in range(CHUNKS):
         for copy in (
@@ -549,8 +516,8 @@
             rcopy(part.at[g, 1, low], fin.at[g, 1, low], s2_send.at[3, g], fin_recv.at[3, g], left),
         ):
             copy.wait_send()
-    for r in range(1, NX):
-        rcopy(ap.at[r], ar.at[r - 1], at_send.at[r - 1], at_recv.at[r - 1], right).wait_send()
+    for copy in attend_copies(0) + attend_copies(1):
+        copy.wait_send()
     for k in range(1, 5):
         for copy in z_copies(k):
             copy.wait_send()
@@ -563,6 +530,28 @@
         for g in range(CHUNKS):
             blocks = buf.at[g, pl.ds(1, BLOCKS - 1)] if g == 0 else buf.at[g]
             rcopy(blocks, blocks, sem.at[0], r_recv.at[g], right).wait_send()
+
+    def collect(n, carry):
+        g = jnp.where(n < 2, n + 2, 3 - n)
+        with jax.named_scope("wait_ret"):
+            pltpu.make_async_copy(ret.at[g], ret.at[g], r_recv.at[g]).wait()
+
+        def store(kq, value):
+            rows_ref[pl.ds(pl.multiple_of(g * GROUP, GROUP), GROUP), kq * width : (kq + 1) * width] = value
+
+        relayout_in(ret, g, store)
+        return carry
+
+    lax.fori_loop(0, CHUNKS, collect, 0)
+    tokens = tok
+    for kq in range(QUARTERS):
+        both = jnp.dot(comb_ref[...], rows_ref[:, kq * width : (kq + 1) * width], preferred_element_type=F32)
+        moe_o[:, kq * width : (kq + 1) * width] = (both[:tokens] + both[tokens:]).astype(BF16)
+
+
+def settle(attn_in, moe_in, attn_o, moe_o):
+    attn_o[...] = attn_in[...]
+    moe_o[...] = moe_in[...]
 
 
 def body(
@@ -623,7 +612,8 @@
             pltpu.VMEM((2 * heads, ta, 2 * vd), F32),
             pltpu.VMEM((NX, ta // NX, heads * vd), BF16),
             pltpu.VMEM((NX, ta // NX, model), BF16),
-            pltpu.VMEM((NX - 1, ta // NX, model), BF16),
+            pltpu.VMEM((2, ta // NX, model // 2), BF16),
+            pltpu.VMEM((2, ta // NX, model), BF16),
             dma((4,)),
             dma((2,)),
             dma((4, 2, 2)),
@@ -646,16 +636,16 @@
             dma((4, CHUNKS)),
             dma((1,)),
             dma((CHUNKS,)),
-            dma((NX - 1,)),
-            dma((NX - 1,)),
+            dma((6,)),
+            dma((6,)),
         ],
         compiler_params=pltpu.CompilerParams(collective_id=0, has_side_effects=True, vmem_limit_bytes=62 * 1024 * 1024),
     )(
         moe_input,
         norm_gain.reshape(1, model),
-        routes,
-        route_weights,
-        queries.reshape(ta, heads * qd),
+        routes.T,
+        route_weights.T,
+        queries,
         keys.reshape(ta, qd),
         values.reshape(ta, vd),
         mix_scale,
@@ -665,7 +655,15 @@
         up_weight[0],
         down_weight[0],
     )
-    return (attn_out, moe_out)
+    return pl.pallas_call(
+        settle,
+        out_shape=(
+            jax.ShapeDtypeStruct(attn_out.shape, BF16),
+            jax.ShapeDtypeStruct(moe_out.shape, BF16),
+        ),
+        in_specs=[vmem] * 2,
+        out_specs=(vmem, vmem),
+    )(attn_out, moe_out)
 
 
 def solution(mesh):

time: 120 us -> 111 us (0.925); the launches traced: 120 us -> 109 us
  local copies, waits for them, and re-layouts: 7.72 us -> 0 us
  Pallas kernels: 112 us -> 109 us
    unnamed x5 -> x0, local copies, waits for them, and re-layouts: 7.72 us -> none
    pallas_call x1, Pallas kernels: 112 us -> 107 us  [body(): pl.pallas_call(kernel, out_shape=(jax.ShapeDtypeStruct((ta // NX, model),...]
    pallas_call x0 -> x1, Pallas kernels: none -> 1.93 us  [body(): pl.pallas_call(settle, out_shape=(jax.ShapeDtypeStruct(attn_out.shape, BF...]
where the time goes in v3:
time: 111 us; the launch traced here: 109 us
  Pallas kernels  109 us (98%)
    pallas_call x1, Pallas kernels, body(): pl.pallas_call(kernel, out_shape=(jax.ShapeDtypeStruct((ta // NX, model),...  107 us

profile of v3, /device:TPU:1, one launch (start us, length us, event | category | flops | bytes accessed | tf_op | source)
XLA Modules:
  0.0 109.2 jit_solution(15184695961027526900)
XLA Ops:
  0.6 106.6 %shard_map.140 = (bf16[48,2048]{1,0:T(8,128)(2,1)}, bf16[96,2048]{1,0:T(8,128)(2,1)}) custom-call(bf16[96,2048]{1,0:T(8,128)(2,1)} %tok_ref.1, f32[1,2048]{1,0:T(1,128)} %bitcast.16, s32[2,96]{1,0:T(2,128)} %bitcast.17, f32[2,96]{1,0:T(2,128)} %bitcast.18, bf16[192,2,128]{2,1,0:T(2,128)(2,1)} %q_in.1, bf16[192,128]{1,0:T(8,128)(2,1)} %bitcast.14, ...), custom_call_target="tpu_custom_call" | custom-call | tf_op jit(solution)/shard_map/pallas_call | solution.py:582
  107.3 1.9 %shard_map.141 = (bf16[48,2048]{1,0:T(8,128)(2,1)}, bf16[96,2048]{1,0:T(8,128)(2,1)}) custom-call(bf16[48,2048]{1,0:T(8,128)(2,1)} %get-tuple-element.4.attn_in, bf16[96,2048]{1,0:T(8,128)(2,1)} %get-tuple-element.5.moe_in), custom_call_target="tpu_custom_call" | custom-call | tf_op jit(solution)/shard_map/pallas_call | solution.py:658

commit v4 on v3

--- a/solution.py
+++ b/solution.py
@@ -27,7 +27,8 @@
     out = [(0, dy, dc) for dy in range(NY) for dc in range(NC)]
     for k in (1, 2, 3):
         out += [(dz, dy, dc) for dc in range(NC) for dy in range(NY) for dz in (k, NZ - k)]
-    return out + [(NZ // 2, dy, dc) for dy in range(NY) for dc in range(NC)]
+    out += [(NZ // 2, dy, dc) for dy in range(NY) for dc in range(NC)]
+    return sum([out[n * BLOCKS : (n + 1) * BLOCKS] for n in (0, 2, 3, 1)], [])
 
 
 OFFSETS = offsets()
@@ -37,7 +38,9 @@
     k = jnp.minimum(dz, NZ - dz)
     ends = dy * NC + dc
     between = 16 * k - 8 + dc * 8 + dy * 2 + (dz > NZ // 2).astype(jnp.int32)
-    return jnp.where(k == 0, ends, jnp.where(k == NZ // 2, 56 + ends, between))
+    place = jnp.where(k == 0, ends, jnp.where(k == NZ // 2, 56 + ends, between))
+    chunk = place >> 4
+    return jnp.where(chunk == 0, 0, jnp.where(chunk == 1, 3, chunk - 1)) * BLOCKS + (place & (BLOCKS - 1))
 
 
 def kernel(
@@ -63,6 +66,8 @@
     outbound,
     q_ref,
     comb_ref,
+    comb_last,
+    sum_ref,
     kbuf,
     vbuf,
     perm,
@@ -84,27 +89,17 @@
     ar,
     w_sem,
     kv_own,
-    z_send,
     z_recv,
-    y_send,
     y_recv,
-    h_send,
     h_recv,
-    c_send,
     c_recv,
     a_send,
     a_recv,
-    x_send,
     x_recv,
-    f_send,
     f_recv,
-    s1_send,
     s1_recv,
-    s2_send,
     fin_recv,
-    b_send,
     r_recv,
-    at_send,
     at_recv,
 ):
     z = lax.axis_index("ep_0")
@@ -188,8 +183,9 @@
         dispatch = dispatch + (slot_iota == slot).astype(F32)
         comb = comb + jnp.where(place_iota == as_col(slot, 0), as_col(rw_ref[k : k + 1, :], 0.0), 0.0)
     high = comb.astype(BF16)
-    comb_ref[:tok] = high
-    comb_ref[tok:] = (comb - high.astype(F32)).astype(BF16)
+    both = jnp.concatenate([high, (comb - high.astype(F32)).astype(BF16)], axis=0)
+    comb_ref[...] = both[:, : slots - GROUP]
+    comb_last[...] = both[:, slots - GROUP :]
     widened = tok_ref[...].astype(F32)
     normed = (
         widened * lax.rsqrt(jnp.mean(widened * widened, axis=1, keepdims=True) + 1e-06) * ng_ref[...]
@@ -216,9 +212,9 @@
         return lax.rem(z + NZ + k, NZ)
 
     def z_copies(k):
-        ups = [rcopy(b.at[zb(1 - k), y, c], b.at[zb(1 - k), y, c], z_send.at[k - 1, 0, j], z_recv.at[k - 1, 0, j], z_up)
+        ups = [rcopy(b.at[zb(1 - k), y, c], b.at[zb(1 - k), y, c], a_send.at[0], z_recv.at[k - 1, 0, j], z_up)
                for _, b, j in kv if k < 4 or j == 0]
-        downs = [rcopy(b.at[zb(k - 1), y, c], b.at[zb(k - 1), y, c], z_send.at[k - 1, 1, j], z_recv.at[k - 1, 1, j], z_down)
+        downs = [rcopy(b.at[zb(k - 1), y, c], b.at[zb(k - 1), y, c], a_send.at[0], z_recv.at[k - 1, 1, j], z_down)
                  for _, b, j in kv if k < 4 or j == 1]
         return ups + downs
 
@@ -231,20 +227,21 @@
             for _, b, j in kv:
                 ref = b.at[zb(dz), y, c]
                 for d, dev in enumerate((y_up, y_down)):
-                    out.append(rcopy(ref, ref, y_send.at[k, n, d, j], y_recv.at[k, n, d, j], dev))
+                    out.append(rcopy(ref, ref, a_send.at[0], y_recv.at[k, n, d, j], dev))
         return out
 
     def hop_copies(k):
         out = []
         for n, dz in enumerate(z_blocks(k)):
             lo = kbuf.at[zb(dz), ym1, c]
-            out.append(rcopy(lo, lo, h_send.at[k, n, 0], h_recv.at[k, n, 0], y_up))
+            out.append(rcopy(lo, lo, a_send.at[0], h_recv.at[k, n, 0], y_up))
             hi = vbuf.at[zb(dz), yp1, c]
-            out.append(rcopy(hi, hi, h_send.at[k, n, 1], h_recv.at[k, n, 1], y_down))
+            out.append(rcopy(hi, hi, a_send.at[0], h_recv.at[k, n, 1], y_down))
         return out
 
-    def core_copies():
-        return [rcopy(b.at[:, :, c], b.at[:, :, c], c_send.at[j], c_recv.at[j], partner) for _, b, j in kv]
+    def core_copies(n):
+        col = lax.rem(y + n, NY)
+        return [rcopy(b.at[:, col, c], b.at[:, col, c], a_send.at[0], c_recv.at[n, j], partner) for _, b, j in kv]
 
     def start(copies):
         for copy in copies:
@@ -274,24 +271,24 @@
             xb[g, 0, :, kq * width : (kq + 1) * width] = value
 
         relayout_in(arr, g, store)
-        rcopy(xb.at[g, 0], xb.at[g, 1], x_send.at[0, g], x_recv.at[0, g], right).start()
-        rcopy(xb.at[g, 0], xb.at[g, 2], x_send.at[1, g], x_recv.at[1, g], left).start()
+        rcopy(xb.at[g, 0], xb.at[g, 1], a_send.at[0], x_recv.at[0, g], right).start()
+        rcopy(xb.at[g, 0], xb.at[g, 2], a_send.at[0], x_recv.at[1, g], left).start()
 
     top, low = pl.ds(0, GROUP // 2), pl.ds(GROUP // 2, GROUP // 2)
 
     def gather_second(g):
-        rcopy(xb.at[g, 0], xb.at[g, 1], x_send.at[0, g], x_recv.at[0, g], right).wait_recv()
-        rcopy(xb.at[g, 1, top], xb.at[g, 3, top], f_send.at[0, g], f_recv.at[0, g], right).start()
-        rcopy(xb.at[g, 0], xb.at[g, 2], x_send.at[1, g], x_recv.at[1, g], left).wait_recv()
-        rcopy(xb.at[g, 2, low], xb.at[g, 3, low], f_send.at[1, g], f_recv.at[1, g], left).start()
+        rcopy(xb.at[g, 0], xb.at[g, 1], a_send.at[0], x_recv.at[0, g], right).wait_recv()
+        rcopy(xb.at[g, 1, top], xb.at[g, 3, top], a_send.at[0], f_recv.at[0, g], right).start()
+        rcopy(xb.at[g, 0], xb.at[g, 2], a_send.at[0], x_recv.at[1, g], left).wait_recv()
+        rcopy(xb.at[g, 2, low], xb.at[g, 3, low], a_send.at[0], f_recv.at[1, g], left).start()
 
     ffe = gw.shape[1]
     model = gw.shape[0]
     rows = NX * GROUP
 
     def experts(g):
-        rcopy(xb.at[g, 1, top], xb.at[g, 3, top], f_send.at[0, g], f_recv.at[0, g], right).wait_recv()
-        rcopy(xb.at[g, 2, low], xb.at[g, 3, low], f_send.at[1, g], f_recv.at[1, g], left).wait_recv()
+        rcopy(xb.at[g, 1, top], xb.at[g, 3, top], a_send.at[0], f_recv.at[0, g], right).wait_recv()
+        rcopy(xb.at[g, 2, low], xb.at[g, 3, low], a_send.at[0], f_recv.at[1, g], left).wait_recv()
 
         @pl.when(g == 0)
         def _():
@@ -311,31 +308,31 @@
             )
 
     def sum_first(g):
-        rcopy(part.at[g, 3, top], opp.at[g, 0], s1_send.at[0, g], s1_recv.at[0, g], right).start()
-        rcopy(part.at[g, 3, low], opp.at[g, 1], s1_send.at[1, g], s1_recv.at[1, g], left).start()
-        rcopy(part.at[g, 2, low], fin.at[g, 0, low], s2_send.at[0, g], fin_recv.at[0, g], right).start()
-        rcopy(part.at[g, 1, top], fin.at[g, 1, top], s2_send.at[1, g], fin_recv.at[1, g], left).start()
+        rcopy(part.at[g, 3, top], opp.at[g, 0], a_send.at[0], s1_recv.at[0, g], right).start()
+        rcopy(part.at[g, 3, low], opp.at[g, 1], a_send.at[0], s1_recv.at[1, g], left).start()
+        rcopy(part.at[g, 2, low], fin.at[g, 0, low], a_send.at[0], fin_recv.at[0, g], right).start()
+        rcopy(part.at[g, 1, top], fin.at[g, 1, top], a_send.at[0], fin_recv.at[1, g], left).start()
 
     def sum_second(g):
-        rcopy(part.at[g, 3, top], opp.at[g, 0], s1_send.at[0, g], s1_recv.at[0, g], right).wait_recv()
+        rcopy(part.at[g, 3, top], opp.at[g, 0], a_send.at[0], s1_recv.at[0, g], right).wait_recv()
         part[g, 2, : GROUP // 2] = (part[g, 2, : GROUP // 2].astype(F32) + opp[g, 0].astype(F32)).astype(BF16)
-        rcopy(part.at[g, 2, top], fin.at[g, 0, top], s2_send.at[2, g], fin_recv.at[2, g], right).start()
-        rcopy(part.at[g, 3, low], opp.at[g, 1], s1_send.at[1, g], s1_recv.at[1, g], left).wait_recv()
+        rcopy(part.at[g, 2, top], fin.at[g, 0, top], a_send.at[0], fin_recv.at[2, g], right).start()
+        rcopy(part.at[g, 3, low], opp.at[g, 1], a_send.at[0], s1_recv.at[1, g], left).wait_recv()
         part[g, 1, GROUP // 2 :] = (part[g, 1, GROUP // 2 :].astype(F32) + opp[g, 1].astype(F32)).astype(BF16)
-        rcopy(part.at[g, 1, low], fin.at[g, 1, low], s2_send.at[3, g], fin_recv.at[3, g], left).start()
+        rcopy(part.at[g, 1, low], fin.at[g, 1, low], a_send.at[0], fin_recv.at[3, g], left).start()
 
     def sum_last(g):
-        rcopy(part.at[g, 2, low], fin.at[g, 0, low], s2_send.at[0, g], fin_recv.at[0, g], right).wait_recv()
-        rcopy(part.at[g, 1, top], fin.at[g, 1, top], s2_send.at[1, g], fin_recv.at[1, g], left).wait_recv()
-        rcopy(part.at[g, 2, top], fin.at[g, 0, top], s2_send.at[2, g], fin_recv.at[2, g], right).wait_recv()
-        rcopy(part.at[g, 1, low], fin.at[g, 1, low], s2_send.at[3, g], fin_recv.at[3, g], left).wait_recv()
+        rcopy(part.at[g, 2, low], fin.at[g, 0, low], a_send.at[0], fin_recv.at[0, g], right).wait_recv()
+        rcopy(part.at[g, 1, top], fin.at[g, 1, top], a_send.at[0], fin_recv.at[1, g], left).wait_recv()
+        rcopy(part.at[g, 2, top], fin.at[g, 0, top], a_send.at[0], fin_recv.at[2, g], right).wait_recv()
+        rcopy(part.at[g, 1, low], fin.at[g, 1, low], a_send.at[0], fin_recv.at[3, g], left).wait_recv()
         total = (part[g, 0].astype(F32) + fin[g, 0].astype(F32) + fin[g, 1].astype(F32)).astype(BF16)
         back[g] = pack(total)
         for i in range(BLOCKS):
             if g == 0 and i == 0:
                 pltpu.make_async_copy(back.at[0, 0], ret.at[0, 0], r_recv.at[0]).start()
             else:
-                rcopy(back.at[g, i], ret.at[g, i], b_send.at[0], r_recv.at[g], from_offset(g * BLOCKS + i)).start()
+                rcopy(back.at[g, i], ret.at[g, i], a_send.at[0], r_recv.at[g], from_offset(g * BLOCKS + i)).start()
 
     ta = q_ref.shape[1]
     span = NY * NC * ta
@@ -384,14 +381,14 @@
     def attend_copies(n):
         if n == 0:
             return [
-                rcopy(ap.at[2, :, one], ao.at[0], at_send.at[0], at_recv.at[0], right),
-                rcopy(ap.at[2, :, two], ao.at[1], at_send.at[1], at_recv.at[1], left),
-                rcopy(ap.at[1, :, two], ar.at[0, :, two], at_send.at[2], at_recv.at[2], right),
-                rcopy(ap.at[3, :, one], ar.at[1, :, one], at_send.at[3], at_recv.at[3], left),
+                rcopy(ap.at[2, :, one], ao.at[0], a_send.at[0], at_recv.at[0], right),
+                rcopy(ap.at[2, :, two], ao.at[1], a_send.at[0], at_recv.at[1], left),
+                rcopy(ap.at[1, :, two], ar.at[0, :, two], a_send.at[0], at_recv.at[2], right),
+                rcopy(ap.at[3, :, one], ar.at[1, :, one], a_send.at[0], at_recv.at[3], left),
             ]
         return [
-            rcopy(ap.at[1, :, one], ar.at[0, :, one], at_send.at[4], at_recv.at[4], right),
-            rcopy(ap.at[3, :, two], ar.at[1, :, two], at_send.at[5], at_recv.at[5], left),
+            rcopy(ap.at[1, :, one], ar.at[0, :, one], a_send.at[0], at_recv.at[4], right),
+            rcopy(ap.at[3, :, two], ar.at[1, :, two], a_send.at[0], at_recv.at[5], left),
         ]
 
     def attend_second():
@@ -409,11 +406,13 @@
         landed(z_copies(1))
         start(z_copies(2))
         start(y_copies(1))
+        send_rows(2)
 
     def kv_2():
         landed(z_copies(2))
         start(z_copies(3))
         start(y_copies(2))
+        send_rows(3)
         landed(y_copies(0))
         start(hop_copies(0))
 
@@ -427,6 +426,7 @@
     def kv_4():
         landed(z_copies(4))
         start(y_copies(4))
+        start(core_copies(0))
         landed(y_copies(2))
         start(hop_copies(2))
 
@@ -434,17 +434,18 @@
         for k in (3, 4):
             landed(y_copies(k))
             start(hop_copies(k))
+        start(core_copies(1))
+        start(core_copies(3))
 
     def kv_6():
         for k in range(5):
             landed(hop_copies(k))
-        start(core_copies())
+        start(core_copies(2))
 
     send_rows(0)
     start(z_copies(1))
     start(y_copies(0))
-    for g in range(1, CHUNKS):
-        send_rows(g)
+    send_rows(1)
     heads = q_in.shape[1]
     map_lane = lax.broadcasted_iota(jnp.int32, (q_in.shape[0], 128), 1) < 64
     with jax.named_scope("q_prep"):
@@ -452,7 +453,13 @@
             scaled = q_in[:, h, :].astype(F32) * 0.125
             q_ref[h] = jnp.where(map_lane, scaled, 0.0).astype(BF16)
             q_ref[heads + h] = jnp.where(map_lane, 0.0, scaled).astype(BF16)
-    run((gather_first, 0), (gather_first, 1), (kv_1,), (gather_second, 0), (gather_first, 2), (kv_2,), (gather_second, 1))
+    run((gather_first, 0), (kv_1,), (gather_second, 0), (gather_first, 1), (kv_2,))
+
+    def attend_begin():
+        for n in range(NY):
+            landed(core_copies(n))
+        m_ref[...] = jnp.full(m_ref.shape, NEG_LARGE, F32)
+        acc_ref[...] = jnp.zeros(acc_ref.shape, F32)
 
     def first_half(s, carry):
         with jax.named_scope("experts"):
@@ -460,43 +467,42 @@
 
         @pl.when(s == 0)
         def _():
-            run((gather_first, 3), (kv_3,), (gather_second, 2))
+            run((sum_first, 0), (gather_second, 1), (gather_first, 2), (kv_3,))
 
         @pl.when(s == 1)
         def _():
-            run((kv_4,), (gather_second, 3))
+            run(
+                (sum_first, 1),
+                (gather_first, 3),
+                (gather_second, 2),
+                (kv_4,),
+                (kv_5,),
+                (kv_6,),
+                (gather_second, 3),
+                (sum_second, 0),
+            )
 
         @pl.when(s == 2)
         def _():
-            run((sum_first, 2), (kv_5,))
+            run((sum_first, 2), (sum_second, 1), (sum_last, 0))
 
         return carry
 
     lax.fori_loop(0, CHUNKS, first_half, 0)
-    run((sum_first, 3), (kv_6,), (sum_second, 2), (sum_first, 1))
-    with jax.named_scope("wait_kv"):
-        landed(core_copies())
-    m_ref[...] = jnp.full(m_ref.shape, NEG_LARGE, F32)
-    acc_ref[...] = jnp.zeros(acc_ref.shape, F32)
-
-    def second_half(s, carry):
-        @pl.when(s < z)
-        def _():
-            with jax.named_scope("attend"):
-                attend_plane(s, False)
-
-        @pl.when(s == 1)
-        def _():
-            run((sum_second, 3), (sum_last, 2), (sum_first, 0))
-
-        @pl.when(s == 4)
-        def _():
-            run((sum_second, 1), (sum_last, 3))
-
-        return carry
-
-    lax.fori_loop(0, NZ - 1, second_half, 0)
-    run((attend_last,), (sum_second, 0), (sum_last, 1), (attend_second,), (sum_last, 0))
+    run(
+        (sum_first, 3),
+        (attend_begin,),
+        (attend_some, 0, 3),
+        (sum_second, 2),
+        (sum_last, 1),
+        (attend_some, 3, 5),
+        (sum_second, 3),
+        (sum_last, 2),
+        (attend_some, 5, NZ),
+        (sum_last, 3),
+        (attend_last,),
+        (attend_second,),
+    )
 
     with jax.named_scope("wait_attn"):
         landed(attend_copies(0)[2:] + attend_copies(1))
@@ -504,16 +510,16 @@
 
     for g in range(CHUNKS):
         for copy in (
-            rcopy(xb.at[g, 0], xb.at[g, 1], x_send.at[0, g], x_recv.at[0, g], right),
-            rcopy(xb.at[g, 0], xb.at[g, 2], x_send.at[1, g], x_recv.at[1, g], left),
-            rcopy(xb.at[g, 1, top], xb.at[g, 3, top], f_send.at[0, g], f_recv.at[0, g], right),
-            rcopy(xb.at[g, 2, low], xb.at[g, 3, low], f_send.at[1, g], f_recv.at[1, g], left),
-            rcopy(part.at[g, 3, top], opp.at[g, 0], s1_send.at[0, g], s1_recv.at[0, g], right),
-            rcopy(part.at[g, 3, low], opp.at[g, 1], s1_send.at[1, g], s1_recv.at[1, g], left),
-            rcopy(part.at[g, 2, low], fin.at[g, 0, low], s2_send.at[0, g], fin_recv.at[0, g], right),
-            rcopy(part.at[g, 1, top], fin.at[g, 1, top], s2_send.at[1, g], fin_recv.at[1, g], left),
-            rcopy(part.at[g, 2, top], fin.at[g, 0, top], s2_send.at[2, g], fin_recv.at[2, g], right),
-            rcopy(part.at[g, 1, low], fin.at[g, 1, low], s2_send.at[3, g], fin_recv.at[3, g], left),
+            rcopy(xb.at[g, 0], xb.at[g, 1], a_send.at[0], x_recv.at[0, g], right),
+            rcopy(xb.at[g, 0], xb.at[g, 2], a_send.at[0], x_recv.at[1, g], left),
+            rcopy(xb.at[g, 1, top], xb.at[g, 3, top], a_send.at[0], f_recv.at[0, g], right),
+            rcopy(xb.at[g, 2, low], xb.at[g, 3, low], a_send.at[0], f_recv.at[1, g], left),
+            rcopy(part.at[g, 3, top], opp.at[g, 0], a_send.at[0], s1_recv.at[0, g], right),
+            rcopy(part.at[g, 3, low], opp.at[g, 1], a_send.at[0], s1_recv.at[1, g], left),
+            rcopy(part.at[g, 2, low], fin.at[g, 0, low], a_send.at[0], fin_recv.at[0, g], right),
+            rcopy(part.at[g, 1, top], fin.at[g, 1, top], a_send.at[0], fin_recv.at[1, g], left),
+            rcopy(part.at[g, 2, top], fin.at[g, 0, top], a_send.at[0], fin_recv.at[2, g], right),
+            rcopy(part.at[g, 1, low], fin.at[g, 1, low], a_send.at[0], fin_recv.at[3, g], left),
         ):
             copy.wait_send()
     for copy in attend_copies(0) + attend_copies(1):
@@ -524,34 +530,36 @@
     for k in range(5):
         for copy in y_copies(k) + hop_copies(k):
             copy.wait_send()
-    for copy in core_copies():
-        copy.wait_send()
-    for sem, buf in ((a_send, outbound), (b_send, back)):
+    for n in range(NY):
+        for copy in core_copies(n):
+            copy.wait_send()
+    def collect(g, carry):
+        with jax.named_scope("wait_ret"):
+            pltpu.make_async_copy(ret.at[g], ret.at[g], r_recv.at[g]).wait()
+
+        def store(kq, value):
+            rows_ref[pl.ds(pl.multiple_of(g * GROUP, GROUP), GROUP), kq * width : (kq + 1) * width] = value
+
+        relayout_in(ret, g, store)
+        return carry
+
+    lax.fori_loop(0, CHUNKS - 1, collect, 0)
+    early = (CHUNKS - 1) * GROUP
+    for kq in range(QUARTERS):
+        cut = slice(kq * width, (kq + 1) * width)
+        both = jnp.dot(comb_ref[...], rows_ref[:early, cut], preferred_element_type=F32)
+        sum_ref[:, cut] = both[:tok] + both[tok:]
+    collect(CHUNKS - 1, 0)
+    with jax.named_scope("combine"):
+        for kq in range(QUARTERS):
+            cut = slice(kq * width, (kq + 1) * width)
+            both = jnp.dot(comb_last[...], rows_ref[early:, cut], preferred_element_type=F32)
+            moe_o[:, cut] = (sum_ref[:, cut] + both[:tok] + both[tok:]).astype(BF16)
+
+    for buf in (outbound, back):
         for g in range(CHUNKS):
             blocks = buf.at[g, pl.ds(1, BLOCKS - 1)] if g == 0 else buf.at[g]
-            rcopy(blocks, blocks, sem.at[0], r_recv.at[g], right).wait_send()
-
-    def collect(n, carry):
-        g = jnp.where(n < 2, n + 2, 3 - n)
-        with jax.named_scope("wait_ret"):
-            pltpu.make_async_copy(ret.at[g], ret.at[g], r_recv.at[g]).wait()
-
-        def store(kq, value):
-            rows_ref[pl.ds(pl.multiple_of(g * GROUP, GROUP), GROUP), kq * width : (kq + 1) * width] = value
-
-        relayout_in(ret, g, store)
-        return carry
-
-    lax.fori_loop(0, CHUNKS, collect, 0)
-    tokens = tok
-    for kq in range(QUARTERS):
-        both = jnp.dot(comb_ref[...], rows_ref[:, kq * width : (kq + 1) * width], preferred_element_type=F32)
-        moe_o[:, kq * width : (kq + 1) * width] = (both[:tokens] + both[tokens:]).astype(BF16)
-
-
-def settle(attn_in, moe_in, attn_o, moe_o):
-    attn_o[...] = attn_in[...]
-    moe_o[...] = moe_in[...]
+            rcopy(blocks, blocks, a_send.at[0], r_recv.at[g], right).wait_send()
 
 
 def body(
@@ -582,8 +590,8 @@
     attn_out, moe_out = pl.pallas_call(
         kernel,
         out_shape=(
-            jax.ShapeDtypeStruct((ta // NX, model), BF16),
-            jax.ShapeDtypeStruct((tok, model), BF16),
+            pltpu.VMEM((ta // NX, model), BF16),
+            pltpu.VMEM((tok, model), BF16),
         ),
         in_specs=[vmem] * 5 + [vmem] * 2 + [pl.BlockSpec(memory_space=pltpu.SMEM), vmem] + [hbm] * 4,
         out_specs=(vmem, vmem),
@@ -594,7 +602,9 @@
             pltpu.VMEM((heads * vd, model), BF16),
             pltpu.VMEM((CHUNKS, BLOCKS, QUARTERS * CAP, width), BF16),
             pltpu.VMEM((2 * heads, ta, qd), BF16),
-            pltpu.VMEM((2 * tok, slots), BF16),
+            pltpu.VMEM((2 * tok, slots - GROUP), BF16),
+            pltpu.VMEM((2 * tok, GROUP), BF16),
+            pltpu.VMEM((tok, model), F32),
             pltpu.VMEM((NZ, NY, NC, ta, qd), BF16),
             pltpu.VMEM((NZ, NY, NC, ta, vd), BF16),
             pltpu.VMEM((size, size), BF16),
@@ -617,26 +627,16 @@
             dma((4,)),
             dma((2,)),
             dma((4, 2, 2)),
-            dma((4, 2, 2)),
-            dma((5, 2, 2, 2)),
             dma((5, 2, 2, 2)),
             dma((5, 2, 2)),
-            dma((5, 2, 2)),
-            dma((2,)),
-            dma((2,)),
+            dma((NY, 2)),
             dma((1,)),
             dma((CHUNKS,)),
             dma((2, CHUNKS)),
             dma((2, CHUNKS)),
             dma((2, CHUNKS)),
-            dma((2, CHUNKS)),
-            dma((2, CHUNKS)),
-            dma((2, CHUNKS)),
             dma((4, CHUNKS)),
-            dma((4, CHUNKS)),
-            dma((1,)),
             dma((CHUNKS,)),
-            dma((6,)),
             dma((6,)),
         ],
         compiler_params=pltpu.CompilerParams(collective_id=0, has_side_effects=True, vmem_limit_bytes=62 * 1024 * 1024),
@@ -655,15 +655,7 @@
         up_weight[0],
         down_weight[0],
     )
-    return pl.pallas_call(
-        settle,
-        out_shape=(
-            jax.ShapeDtypeStruct(attn_out.shape, BF16),
-            jax.ShapeDtypeStruct(moe_out.shape, BF16),
-        ),
-        in_specs=[vmem] * 2,
-        out_specs=(vmem, vmem),
-    )(attn_out, moe_out)
+    return (attn_out, moe_out)
 
 
 def solution(mesh):

time: 111 us -> 108 us (0.973); the launches traced: 109 us -> 108 us
  Pallas kernels: 109 us -> 106 us
  local copies, waits for them, and re-layouts: 0 us -> 1.42 us
    pallas_call x2 -> x1, Pallas kernels: 109 us -> 106 us  [body(): pl.pallas_call(kernel, out_shape=(pltpu.VMEM((ta // NX, model), BF16), pl...]
    unnamed x0 -> x2, local copies, waits for them, and re-layouts: none -> 1.42 us
where the time goes in v4:
time: 108 us
  Pallas kernels  106 us (98%)
  local copies, waits for them, and re-layouts  1.42 us (1%)
    pallas_call x1, Pallas kernels, body(): pl.pallas_call(kernel, out_shape=(pltpu.VMEM((ta // NX, model), BF16), pl...  106 us

profile of v4, /device:TPU:1, one launch (start us, length us, event | category | flops | bytes accessed | tf_op | source)
XLA Modules:
  0.0 108.1 jit_solution(5429121739257993418)
XLA Ops:
  0.6 106.0 %shard_map.140 = (bf16[48,2048]{1,0:T(8,128)(2,1)S(1)}, bf16[96,2048]{1,0:T(8,128)(2,1)S(1)}) custom-call(bf16[96,2048]{1,0:T(8,128)(2,1)} %tok_ref.1, f32[1,2048]{1,0:T(1,128)} %bitcast.16, s32[2,96]{1,0:T(2,128)} %bitcast.17, f32[2,96]{1,0:T(2,128)} %bitcast.18, bf16[192,2,128]{2,1,0:T(2,128)(2,1)} %q_in.1, bf16[192,128]{1,0:T(8,128)(2,1)} %bitcast.14, ...), custom_call_target="tpu_custom_call" | custom-call | tf_op jit(solution)/shard_map/pallas_call | solution.py:590
  106.6 0.7 copy.17
  107.3 0.7 copy.18
